TPU v7x, 512 devices: a whole 4x4x16 slice. The times are simulated.
512 devices in a mesh: sp: 64 (over z, y), tp: 8 (over x, core).
Axes of the slice: x: 4, y: 4, z: 16, core: 2. Of those that a mesh axis runs over, the one named last changes fastest.
Arguments:
- tokens: bfloat16 [16384, 2048], P('sp', 'tp'), may hold values from -6 to 6
- norm_gain: float32 [2048], replicated, may hold values from 0.1 to 1.9
- recv_weight: bfloat16 [2048, 1024], P(None, 'tp'), may hold values from -0.125 to 0.125
- lin_key_weight: bfloat16 [2048, 1024], P(None, 'tp'), may hold values from -0.125 to 0.125
- lin_value_weight: bfloat16 [2048, 1024], P(None, 'tp'), may hold values from -0.125 to 0.125
- decay_down: bfloat16 [2048, 64], replicated, may hold values from -0.125 to 0.125
- decay_up: bfloat16 [64, 1024], P(None, 'tp'), may hold values from -0.75 to 0.75
- decay_log_bias: float32 [1024], P('tp'), may hold values from -13 to -3
- decay_shift: float32 [16384, 1024], P('sp', 'tp'), may hold values from -1 to 13
- learn_rate: float32 [1024], P('tp'), may hold values from 0 to 1
- group_gain: float32 [1024], P('tp'), may hold values from 0.1 to 1.9
- initial_state: float32 [16, 64, 64], P('tp'), may hold values from -768 to 768
- query_weight: bfloat16 [2048, 1024], P(None, 'tp'), may hold values from -8 to 8
- att_key_weight: bfloat16 [2048, 1024], P(None, 'tp'), may hold values from -1 to 1
- att_value_weight: bfloat16 [2048, 1024], P(None, 'tp'), may hold values from -0.125 to 0.125
- gate_cache: float32 [16384, 8], P('sp', 'tp'), may hold values from -16384 to 0, as said below
- att_gain: float32 [1024], P('tp'), may hold values from 0.1 to 1.9
- out_lin_weight: bfloat16 [1024, 2048], P('tp'), may hold values from -0.125 to 0.125
- out_att_weight: bfloat16 [1024, 2048], P('tp'), may hold values from -0.125 to 0.125
Outputs:
- mixed_out: bfloat16 [16384, 2048], P('sp', 'tp')
Inputs may be any that keep to these rules, and one draw needn't show every extreme that they name: `gate_cache`: never rises along the sequence.
All inputs are finite; a program needn't handle non-finite values.
Results may differ from a plain program's by a relative error of at most 0.025.
Values may be sent and summed in bfloat16 or wider, within the bound.
No kernel may reach another device: no remote copies, remote signals or barrier semaphores. Data moves between devices by JAX's collectives and lax.ppermute only.
A program may use at most 64 MiB of HBM per device.

v0:
```python
import functools
import math

import jax
import jax.numpy as jnp
from jax import lax
from jax.experimental import pallas as pl
from jax.experimental.pallas import tpu as pltpu
from jax.sharding import Mesh
from jax.sharding import PartitionSpec as P

HEAD_LIN = 64
HEAD_ATT = 128
WIDE = 128
KEYS = ("zh", "zl")
SP = KEYS + ("near",)
TP = ("x", "c")
LOG2E = math.log2(math.e)
NEG = -1e30
F32 = jnp.float32
BF16 = jnp.bfloat16


def params(mib):
    return pltpu.CompilerParams(vmem_limit_bytes=mib * 1024 * 1024)


def cost(flops, size):
    return pl.CostEstimate(flops=flops, bytes_accessed=size, transcendentals=0)


def dot(a, b, dims=((1,), (0,))):
    return lax.dot_general(a, b, (dims, ((), ())), preferred_element_type=F32)


def parts_of(a):
    high = a.astype(BF16)
    return high, (a - high.astype(F32)).astype(BF16)


def dot3(a, b, dims=((1,), (0,))):
    ah, al = parts_of(a)
    bh, bl = parts_of(b)
    return dot(ah, bh, dims) + (dot(ah, bl, dims) + dot(al, bh, dims))


def dot2(a, b, dims=((1,), (0,))):
    ah, al = parts_of(a)
    return dot(ah, b, dims) + dot(al, b, dims)


def in_thirds(a):
    high, mid = parts_of(a)
    low = (a - high.astype(F32) - mid.astype(F32)).astype(BF16)
    return jnp.concatenate([high, mid, low, jnp.zeros((10, WIDE), BF16)], axis=0)


def iota(shape, dim):
    return lax.broadcasted_iota(jnp.int32, shape, dim)


def by_head(a):
    left = iota(a.shape, 1) < HEAD_LIN
    first = jnp.sum(jnp.where(left, a, 0.0), axis=1, keepdims=True)
    second = jnp.sum(jnp.where(left, 0.0, a), axis=1, keepdims=True)
    return jnp.where(left, first, second)


def scaled_pieces(place_ref, own_ref, other_ref, gain_ref):
    shards, rows, depth = own_ref.shape
    core = place_ref[3]
    scaled, squares = [], jnp.zeros((rows, depth), F32)
    for c, ref in enumerate((own_ref, other_ref)):
        for j in range(shards):
            start = pl.multiple_of((2 * j + (core if c == 0 else 1 - core)) * depth, depth)
            wide = ref[j].astype(F32)
            scaled.append(((wide * gain_ref[:, pl.ds(start, depth)]).astype(BF16), start))
            squares = squares + wide * wide
    mean = jnp.sum(squares, axis=1, keepdims=True) / (2 * shards * depth)
    return scaled, lax.rsqrt(mean + 1e-6)


def projected(scaled, inverse, *w_refs):
    total = 0.0
    for piece, start in scaled:
        weight = [w_ref[pl.ds(start, piece.shape[1])] for w_ref in w_refs]
        total = total + dot(piece, jnp.concatenate(weight, axis=1))
    return total * inverse


def spread_kernel(place_ref, tokens_ref, out_ref):
    tokens = tokens_ref[...]
    for j in range(out_ref.shape[0]):
        out_ref[j] = tokens


def kv_kernel(place_ref, own_ref, other_ref, gain_ref, wk_ref, wv_ref, out_ref):
    scaled, inverse = scaled_pieces(place_ref, own_ref, other_ref, gain_ref)
    rows = own_ref.shape[1]
    both = projected(scaled, inverse, wk_ref, wv_ref).astype(BF16)
    out_ref[0:rows] = both[:, :HEAD_ATT]
    out_ref[rows:] = both[:, HEAD_ATT:]


def spans(log_decay):
    rows = log_decay.shape[0]
    row = iota(log_decay.shape, 0)
    zero = jnp.zeros_like(log_decay)
    before = [None] + [pltpu.roll(log_decay, i, 0) for i in range(1, 8)]
    behind = [None] + [pltpu.roll(log_decay, rows - i, 0) for i in range(1, 8)]
    ahead, after = {1: zero}, {1: zero}
    for h in (2, 4, 8):
        place = row & (h - 1)
        a, b = zero, zero
        for i in range(1, h):
            a = a + jnp.where(place >= i, before[i], 0.0)
            b = b + jnp.where(place + i < h, behind[i], 0.0)
        ahead[h], after[h] = a, b
    h = 8
    while h < rows:
        shape = (rows // (2 * h), 2 * h, WIDE)
        a, b = ahead[h].reshape(shape), after[h].reshape(shape)
        step = log_decay.reshape(shape)
        left = a[:, h - 1 : h] + step[:, h - 1 : h]
        right = b[:, h : h + 1] + step[:, h : h + 1]
        a = jnp.concatenate([a[:, :h], a[:, h:] + left], axis=1)
        b = jnp.concatenate([b[:, :h] + right, b[:, h:]], axis=1)
        h *= 2
        ahead[h], after[h] = a.reshape(rows, WIDE), b.reshape(rows, WIDE)
    return ahead, after


def lin_kernel(
    place_ref,
    own_ref,
    other_ref,
    gain_ref,
    wr_ref,
    wk_ref,
    wv_ref,
    wq_ref,
    down_ref,
    up_ref,
    bias_ref,
    shift_ref,
    rate_ref,
    gate_ref,
    send_ref,
    gates_ref,
    reach_ref,
    local_ref,
    pairs_ref,
):
    scaled, inverse = scaled_pieces(place_ref, own_ref, other_ref, gain_ref)
    rows = shift_ref.shape[0]
    both = projected(scaled, inverse, wr_ref, wk_ref).astype(BF16)
    recv, key = both[:, :WIDE].astype(F32), both[:, WIDE:].astype(F32)
    both = projected(scaled, inverse, wv_ref, wq_ref).astype(BF16)
    value = both[:, :WIDE]
    send_ref[0, 0:rows] = both[:, WIDE:]
    low = 0.0
    for piece, start in scaled:
        low = low + dot(piece, down_ref[:, pl.ds(start, piece.shape[1])], ((1,), (1,)))
    low = (low * inverse).astype(BF16).astype(F32)
    exponent = bias_ref[...] + shift_ref[...] + dot(jnp.tanh(low).astype(BF16), up_ref[...])
    log_decay = -jnp.exp(exponent)
    unit = key * lax.rsqrt(by_head(key * key) + 1e-6)
    rate = unit * rate_ref[...]

    ahead, after = spans(log_decay)
    half = rows // 2
    lane = iota((rows, WIDE), 1)
    row = iota((rows, WIDE), 0)
    tall = iota((half, half), 0)
    flat = iota((half, half), 1)
    heads = [lane < HEAD_LIN, lane >= HEAD_LIN]
    eye = tall == flat
    blocks = slice(0, half), slice(half, rows)

    def of_heads(a):
        return [jnp.where(mine, a, 0.0).astype(BF16) for mine in heads]

    def below(h):
        level = h.bit_length()
        near = (tall >> level) == (flat >> level)
        return near & ((tall & h) != 0) & ((flat & h) == 0)

    for m, source in enumerate((key, rate)):
        now = by_head(recv * source)
        for n in range(2):
            for b in range(2):
                cols = slice(m * rows + b * half, m * rows + (b + 1) * half)
                same_row = now[blocks[b], n * HEAD_LIN : n * HEAD_LIN + 1]
                pairs_ref[n, 1, blocks[b], cols] = jnp.where(eye, same_row, 0.0)
                pairs_ref[n, 0, blocks[b], cols] = jnp.zeros((half, half), F32)
            cols = slice(m * rows + half, (m + 1) * rows)
            for k in range(2):
                pairs_ref[n, k, blocks[0], cols] = jnp.zeros((half, half), F32)
    h = 1
    while h < rows:
        late = (row & h) != 0
        to_u = jnp.where(late, jnp.exp(ahead[h]), 0.0)
        to_q = jnp.where(late, jnp.exp(ahead[h] + log_decay), 0.0)
        from_s = jnp.where(late, 0.0, jnp.exp(after[h]))
        right = (key * from_s).astype(BF16), (rate * from_s).astype(BF16)
        left = of_heads(unit * to_u) + of_heads(recv * to_q)
        for b in range(2) if h < half else (1,):
            c = b if h < half else 0
            product = dot(
                jnp.concatenate([a[blocks[b]] for a in left], axis=0),
                jnp.concatenate([a[blocks[c]] for a in right], axis=0),
                ((1,), (1,)),
            )
            for k in range(2):
                for n in range(2):
                    for m in range(2):
                        cols = slice(m * rows + c * half, m * rows + (c + 1) * half)
                        new = product[
                            (2 * k + n) * half : (2 * k + n + 1) * half,
                            m * half : (m + 1) * half,
                        ]
                        if h < half:
                            new = jnp.where(below(h), new, pairs_ref[n, k, blocks[b], cols])
                        pairs_ref[n, k, blocks[b], cols] = new
        h *= 2

    solved = {}
    h = 1
    while h < half:
        here = below(h)
        for n in range(2):
            for b in range(2):
                cols = slice(rows + b * half, rows + (b + 1) * half)
                links = jnp.where(here, pairs_ref[n, 0, blocks[b], cols], 0.0)
                if h == 1:
                    solved[n, b] = jnp.where(eye, 1.0, 0.0) - links
                else:
                    step = dot3(links, solved[n, b])
                    solved[n, b] = solved[n, b] - dot3(solved[n, b], step)
        h *= 2

    full_u = unit * jnp.exp(ahead[rows])
    full_q = recv * jnp.exp(ahead[rows] + log_decay)
    tail = jnp.exp(after[rows])
    full_k = key * tail
    full_r = rate * tail
    reach, local, moved = [], [], []
    for n in range(2):
        add = dot2(pairs_ref[n, 0, :, :rows], value)
        source = jnp.where(heads[n], full_u, pltpu.roll(add, HEAD_LIN, 1))
        first = dot3(solved[n, 0], source[:half])
        later = source[half:] - dot3(pairs_ref[n, 0, half:, rows : rows + half], first)
        along = jnp.concatenate([first, dot3(solved[n, 1], later)], axis=0)
        taken = dot3(pairs_ref[n, 1, :, rows:], along)
        reach.append(full_q - taken)
        local.append(dot2(pairs_ref[n, 1, :, :rows], value) - pltpu.roll(taken, HEAD_LIN, 1))
        moved.append(dot3(along, full_r, ((0,), (0,))))
    reach_ref[...] = jnp.where(heads[0], reach[0], reach[1])
    local_ref[...] = jnp.where(heads[0], local[0], local[1])

    lane = iota((WIDE, WIDE), 1)
    row = iota((WIDE, WIDE), 0)
    same = (lane < HEAD_LIN) == (row < HEAD_LIN)
    added = pltpu.roll(dot2(full_k, value, ((0,), (0,))).T, HEAD_LIN, 0)
    last = jnp.exp(ahead[rows][rows - 1 : rows] + log_decay[rows - 1 : rows]) - 1.0
    packed = jnp.where(same, jnp.where(lane == row, last, 0.0), added)
    packed = packed - jnp.where(lane < HEAD_LIN, moved[0], moved[1])
    send_ref[0, rows : rows + WIDE] = packed.astype(BF16)
    gates = in_thirds(gate_ref[...])
    send_ref[0, rows + WIDE :] = gates
    gates_ref[...] = gates
    whole = send_ref[0]
    for j in range(1, send_ref.shape[0]):
        send_ref[j] = whole


def unpacked(packed):
    packed = packed.astype(F32)
    lane = iota((WIDE, WIDE), 1)
    row = iota((WIDE, WIDE), 0)
    same = (lane < HEAD_LIN) == (row < HEAD_LIN)
    return jnp.where(same, packed, 0.0), jnp.where(same, pltpu.roll(packed, HEAD_LIN, 0), 0.0)


def repacked(total):
    lane = iota((WIDE, WIDE), 1)
    row = iota((WIDE, WIDE), 0)
    same = (lane < HEAD_LIN) == (row < HEAD_LIN)
    return jnp.where(same, total[0], pltpu.roll(total[1], HEAD_LIN, 0)).astype(BF16)


def chained(first, second):
    return (
        first[0] + second[0] + dot3(first[0], second[0]),
        first[1] + second[1] + dot3(first[1], second[0]),
    )


def row_kernel(place_ref, gathered_ref, gates_ref, send_ref, before_ref, *, rows):
    near = place_ref[2]
    count = gathered_ref.shape[0]
    total = mine = jnp.zeros((WIDE, WIDE), F32), jnp.zeros((WIDE, WIDE), F32)
    for j in range(count):
        mine = tuple(jnp.where(near == j, t, m) for t, m in zip(total, mine))
        here = unpacked(gathered_ref[j, rows : rows + WIDE])
        total = chained(total, here) if j else here
    before_ref[0], before_ref[1] = mine
    send_ref[0:WIDE] = repacked(total)
    send_ref[WIDE:] = gates_ref[...]


def mix_kernel(place_ref, state_ref, gathered_ref, before_ref, reach_ref, local_ref, gain_ref, out_ref):
    none = jnp.zeros((HEAD_LIN, HEAD_LIN), F32)
    state = jnp.concatenate(
        [
            jnp.concatenate([state_ref[0], none], axis=1),
            jnp.concatenate([none, state_ref[1]], axis=1),
        ],
        axis=0,
    )

    def step(k, state):
        packed = gathered_ref[k]
        moved, added = unpacked(packed[0:WIDE])
        return state + dot2(state, moved.astype(BF16)) + added

    state = lax.fori_loop(0, place_ref[0] * 2 + place_ref[1], step, state)
    state = state + dot3(state, before_ref[0]) + before_ref[1]
    raw = dot3(reach_ref[...], state, ((1,), (1,))) + local_ref[...]
    off = raw - by_head(raw) * (1.0 / HEAD_LIN)
    spread = by_head(off * off) * (1.0 / HEAD_LIN)
    out_ref[...] = (off * lax.rsqrt(spread + 0.00064) * gain_ref[...]).astype(BF16)


def joined(gates):
    gates = gates.astype(F32)
    return gates[0:2] + gates[2:4] + gates[4:6]


def att_kernel(
    place_ref, asked_ref, held_ref, keys_ref, out_ref, logit_ref, best_ref, sum_ref, *, rows
):
    z, y = place_ref[0] * 2 + place_ref[1], place_ref[2]
    count = asked_ref.shape[0]
    scale = HEAD_ATT ** (-0.5) * LOG2E
    best_ref[...] = jnp.full(best_ref.shape, NEG, F32)
    sum_ref[...] = jnp.zeros(sum_ref.shape, F32)
    ones = jnp.ones((rows, HEAD_ATT), BF16)
    base = joined(asked_ref[0, rows + WIDE : rows + WIDE + 16])[0:1, 0:1]

    def score(k, masked):
        key = keys_ref[k, 0:rows]
        drop = (base - joined(held_ref[k, WIDE : WIDE + 16])) * LOG2E
        drop = jnp.concatenate([drop[0:1], drop[1:2]], axis=1)
        for j in range(count):
            logits = dot(asked_ref[j, 0:rows], key, ((1,), (1,))) * scale + drop
            if masked:
                allowed = y * rows + iota(logits.shape, 1) <= j * rows + iota(logits.shape, 0)
                logits = jnp.where(allowed, logits, NEG)
            logit_ref[k, j] = logits
            top = functools.reduce(
                jnp.maximum, [logits[:, i : i + WIDE] for i in range(0, rows, WIDE)]
            )
            best_ref[j] = jnp.maximum(best_ref[j], top)

    def gather(*blocks):
        value = [jnp.concatenate([keys_ref[k, rows:], ones], axis=1) for k in blocks]
        for j in range(count):
            best = jnp.concatenate([best_ref[j]] * (rows // WIDE), axis=1)
            new = 0.0
            for k, v in zip(blocks, value):
                new = new + dot(jnp.exp2(logit_ref[k, j] - best).astype(BF16), v)
            sum_ref[j] = sum_ref[j] + new

    def score_many(i, carry):
        for k in range(3):
            score(3 * i + k, False)
        return carry

    def score_one(k, carry):
        score(k, False)
        return carry

    def gather_many(i, carry):
        gather(*(4 * i + k for k in range(4)))
        return carry

    def gather_one(k, carry):
        gather(k)
        return carry

    many = z // 3
    lax.fori_loop(0, many, score_many, 0)
    lax.fori_loop(3 * many, z, score_one, 0)
    score(z, True)
    for j in range(count):
        best = jnp.max(best_ref[j], axis=1, keepdims=True)
        best = jnp.where(best > 0.5 * NEG, best, 0.0)
        best_ref[j] = jnp.broadcast_to(best, best_ref.shape[1:])
    many = (z + 1) // 4
    lax.fori_loop(0, many, gather_many, 0)
    lax.fori_loop(4 * many, z + 1, gather_one, 0)
    eye = iota((WIDE, WIDE), 0) == iota((WIDE, WIDE), 1)
    for j in range(count):
        total = sum_ref[j, :, HEAD_ATT:]
        some = total > 0.0
        safe = jnp.where(some, total, 1.0)
        out_ref[j, 0:rows] = (sum_ref[j, :, 0:HEAD_ATT] / safe).astype(BF16)
        level = jnp.where(some, best_ref[j] + jnp.log(safe) * LOG2E, NEG)
        level = [
            jnp.sum(jnp.where(eye, level[i : i + WIDE], 0.0), axis=0, keepdims=True)
            for i in range(0, rows, WIDE)
        ]
        out_ref[j, rows:] = in_thirds(jnp.concatenate(level, axis=0))


def out_kernel(place_ref, parts_ref, lin_ref, gain_ref, wl_ref, wa_ref, own_ref, other_ref):
    count, rows = parts_ref.shape[0], lin_ref.shape[0]
    core = place_ref[3]
    levels = [joined(parts_ref[j, rows:]) for j in range(count)]
    top = functools.reduce(jnp.maximum, levels)
    shares = [jnp.exp2(level - top) for level in levels]
    total = functools.reduce(jnp.add, shares)
    shares = jnp.concatenate([share / total for share in shares], axis=0).T
    raw = []
    for i in range(rows // WIDE):
        mine = slice(i * WIDE, (i + 1) * WIDE)
        raw.append(
            functools.reduce(
                jnp.add,
                [
                    shares[:, 2 * j + i : 2 * j + i + 1] * parts_ref[j, mine].astype(F32)
                    for j in range(count)
                ],
            )
        )
    raw = jnp.concatenate(raw, axis=0)
    size = jnp.mean(raw * raw, axis=1, keepdims=True)
    att = (raw * lax.rsqrt(size + 1e-6) * gain_ref[...]).astype(BF16)
    lin = lin_ref[...]
    width = own_ref.shape[2]
    for c, ref in enumerate((own_ref, other_ref)):
        for j in range(ref.shape[0]):
            start = pl.multiple_of((2 * j + (core if c == 0 else 1 - core)) * width, width)
            mine = pl.ds(start, width)
            ref[j] = (dot(lin, wl_ref[:, mine]) + dot(att, wa_ref[:, mine])).astype(BF16)


def to_partner(a, axis):
    return lax.ppermute(a, axis, [(0, 1), (1, 0)])


def smem():
    return pl.BlockSpec(memory_space=pltpu.SMEM)


def vmem():
    return pl.BlockSpec(memory_space=pltpu.VMEM)


def call(kernel, name, shapes, flops, size, mib, scratch=()):
    def run(*operands):
        many = isinstance(shapes, (list, tuple))
        return pl.pallas_call(
            kernel,
            name=name,
            out_shape=shapes,
            in_specs=[smem()] + [vmem()] * (len(operands) - 1),
            out_specs=[vmem()] * len(shapes) if many else vmem(),
            scratch_shapes=list(scratch),
            compiler_params=params(mib),
            cost_estimate=cost(flops, size),
        )(*operands)

    return run


def body(
    tokens,
    norm_gain,
    recv_weight,
    lin_key_weight,
    lin_value_weight,
    decay_down,
    decay_up,
    decay_log_bias,
    decay_shift,
    learn_rate,
    group_gain,
    initial_state,
    query_weight,
    att_key_weight,
    att_value_weight,
    gate_cache,
    att_gain,
    out_lin_weight,
    out_att_weight,
):
    rows = tokens.shape[0]
    nz, ny, nx = (lax.axis_size(axis) for axis in (KEYS, "near", "x"))
    model_width = norm_gain.shape[0]
    shape = jax.ShapeDtypeStruct
    place = jnp.stack([lax.axis_index(axis) for axis in SP + ("c",)]).astype(jnp.int32)
    gain = norm_gain.reshape(1, -1)

    copies = call(spread_kernel, "spread", shape((nx, *tokens.shape), BF16), 10**10, 1 << 24, 4)(
        place, tokens
    )
    own = lax.all_to_all(copies, "x", 0, 0, tiled=True)
    other = to_partner(own, "c")
    kv = call(
        kv_kernel, "kv", shape((2 * rows, WIDE), BF16), 2 * rows * model_width * 256, 1 << 21, 12
    )(place, own, other, gain, att_key_weight, att_value_weight)
    keys = lax.all_gather(kv, KEYS)

    extra = 16
    send, gates, reach, local = call(
        lin_kernel,
        "lin",
        (
            shape((ny, rows + WIDE + extra, WIDE), BF16),
            shape((extra, WIDE), BF16),
            shape((rows, WIDE), F32),
            shape((rows, WIDE), F32),
        ),
        4 * 10**9,
        1 << 22,
        24,
        scratch=[pltpu.VMEM((2, 2, rows, 2 * rows), F32)],
    )(
        place,
        own,
        other,
        gain,
        recv_weight,
        lin_key_weight,
        lin_value_weight,
        query_weight,
        decay_down.T,
        decay_up,
        decay_log_bias.reshape(1, -1),
        decay_shift,
        learn_rate.reshape(1, -1),
        gate_cache.reshape(rows // WIDE, WIDE),
    )
    asked = lax.all_to_all(send, "near", 0, 0, tiled=True)
    row_send, before = call(
        functools.partial(row_kernel, rows=rows),
        "row",
        (shape((WIDE + extra, WIDE), BF16), shape((2, WIDE, WIDE), F32)),
        10**8,
        1 << 20,
        12,
    )(place, asked, gates)
    held = lax.all_gather(row_send, KEYS)
    lin_mixed = call(mix_kernel, "mix", shape((rows, WIDE), BF16), 10**9, 1 << 20, 12)(
        place, initial_state, held, before, reach, local, group_gain.reshape(1, -1)
    )
    found = call(
        functools.partial(att_kernel, rows=rows),
        "att",
        shape((ny, rows + extra, HEAD_ATT), BF16),
        ny * rows * nz * rows * 512,
        1 << 22,
        36,
        scratch=[
            pltpu.VMEM((nz, ny, rows, rows), F32),
            pltpu.VMEM((ny, rows, WIDE), F32),
            pltpu.VMEM((ny, rows, HEAD_ATT + WIDE), F32),
        ],
    )(place, asked, held, keys)
    parts = lax.all_to_all(found, "near", 0, 0, tiled=True)
    width = model_width // (2 * nx)
    tile = shape((nx, rows, width), BF16)
    mine, theirs = call(
        out_kernel, "out", (tile, tile), 2 * rows * 256 * model_width, 1 << 21, 12
    )(place, parts, lin_mixed, att_gain.reshape(1, -1), out_lin_weight, out_att_weight)
    pair = (mine.astype(F32) + to_partner(theirs, "c").astype(F32)).astype(BF16)
    tiles = lax.all_to_all(pair, "x", 0, 0, tiled=True)
    return jnp.sum(tiles.astype(F32), axis=0).astype(BF16)


def solution(mesh):
    sp, tp = mesh.shape["sp"], mesh.shape["tp"]
    cores = 2
    near = math.isqrt(sp) if sp > 16 else 2
    torus = Mesh(mesh.devices.reshape(sp // (2 * near), 2, near, tp // cores, cores), SP + TP)
    return jax.shard_map(
        body,
        mesh=torus,
        in_specs=(
            P(SP, TP),
            P(),
            P(None, TP),
            P(None, TP),
            P(None, TP),
            P(),
            P(None, TP),
            P(TP),
            P(SP, TP),
            P(TP),
            P(TP),
            P(TP, None, None),
            P(None, TP),
            P(None, TP),
            P(None, TP),
            P(SP, TP),
            P(TP),
            P(TP, None),
            P(TP, None),
        ),
        out_specs=P(SP, TP),
        check_vma=False,
    )
```

profile of v0, /device:TPU:1, one launch (start us, length us, event | category | flops | bytes accessed | tf_op | source)
XLA Modules:
  0.0 147.1 jit_solution(4187151630368996206)
XLA Ops:
  6.5 0.1 pad_add_fusion.place_ref
  6.6 0.9 copy-done.12
  7.5 0.0 copy-start.15
  7.5 0.0 copy-start.17
  7.6 0.0 copy-start.18
  7.6 0.6 spread.1
  8.1 0.0 copy-start.7
  8.2 0.0 copy-start.8
  8.2 11.7 %all_to_all.20.own_ref = bf16[4,256,256]{2,1,0:T(8,128)(2,1)S(1)} all-to-all(bf16[4,256,256]{2,1,0:T(8,128)(2,1)S(1)} %spread.1), channel_id=1, replica_groups=mesh['zh'=4,'zl'=2,'near'=8,'x'=4,'c'=2] {'x'}, dimensions={0} | all-to-all | bytes 1048576 | tf_op jit(solution)/shard_map/all_to_all | solution.py:509
  19.9 7.8 %collective-permute-start = (bf16[4,256,256]{2,1,0:T(8,128)(2,1)S(1)}, bf16[4,256,256]{2,1,0:T(8,128)(2,1)S(1)}, u32[]{:S(2)}, u32[]{:S(2)}) collective-permute-start(bf16[4,256,256]{2,1,0:T(8,128)(2,1)S(1)} %all_to_all.20.own_ref), channel_id=1, source_target_pairs={{0,1},{1,0},{2,3},{3,2},{4,5},{5,4},{6,7},{7,6},{8,9},{9,8},{10,11... | collective-permute-start | bytes 1572872 | tf_op jit(solution)/shard_map/ppermute | solution.py:450
  27.7 1.5 %collective-permute-done.other_ref = bf16[4,256,256]{2,1,0:T(8,128)(2,1)S(1)} collective-permute-done((bf16[4,256,256]{2,1,0:T(8,128)(2,1)S(1)}, bf16[4,256,256]{2,1,0:T(8,128)(2,1)S(1)}, u32[]{:S(2)}, u32[]{:S(2)}) %collective-permute-start) | collective-permute-done | bytes 524320 | tf_op jit(solution)/shard_map/ppermute | solution.py:450
  29.2 0.0 copy-done.9
  29.2 0.0 copy-done.10
  29.2 0.0 copy-done.11
  29.2 0.0 copy-done.13
  29.2 0.0 copy-done.15
  29.2 0.0 copy-done.17
  29.2 0.0 copy-done.18
  29.2 0.0 copy-done.7
  29.2 0.0 copy-done.8
  29.3 0.0 copy-done.4
  29.3 0.6 copy-done.16
  29.9 8.7 %lin.1 = (bf16[8,400,128]{2,1,0:T(8,128)(2,1)}, bf16[16,128]{1,0:T(8,128)(2,1)S(1)}, f32[256,128]{1,0:T(8,128)S(1)}, f32[256,128]{1,0:T(8,128)S(1)}) custom-call(s32[4]{0:T(128)S(1)} %pad_add_fusion.place_ref, bf16[4,256,256]{2,1,0:T(8,128)(2,1)S(1)} %all_to_all.20.own_ref, bf16[4,256,256]{2,1,0:T(8,128)(2,1)S(1)} %collective-permute-done.other_ref, ...), custom_call_target="tpu_custom_call" | custom-call | flops 4000000000 | bytes 4194304 | tf_op jit(solution)/shard_map/lin/pallas_call | solution.py:464
  38.5 3.7 %all-to-all-start.1 = ((bf16[8,400,128]{2,1,0:T(8,128)(2,1)}), bf16[8,400,128]{2,1,0:T(8,128)(2,1)S(1)}, u32[]{:S(2)}, u32[]{:S(2)}) async-start(bf16[8,400,128]{2,1,0:T(8,128)(2,1)} %get-tuple-element.13), calls=%async_computation.1 | async-start | bytes 1638400 | tf_op jit(solution)/shard_map/all_to_all | solution.py:546
  42.2 0.0 all-gather.4.cloned.1.call-start
  42.3 0.0 copy-done
  42.3 0.0 copy-done.1
  42.3 1.7 %kv.1 = bf16[512,128]{1,0:T(8,128)(2,1)} custom-call(s32[4]{0:T(128)S(1)} %pad_add_fusion.place_ref, bf16[4,256,256]{2,1,0:T(8,128)(2,1)S(1)} %all_to_all.20.own_ref, bf16[4,256,256]{2,1,0:T(8,128)(2,1)S(1)} %collective-permute-done.other_ref, f32[1,2048]{1,0:T(1,128)S(1)} %bitcast.16, bf16[2048,128]{1,0:T(8,128)(2,1)S(1)} %copy-done, ...), custom_call_target="tpu_custom_call" | custom-call | flops 268435456 | bytes 2097152 | tf_op jit(solution)/shard_map/kv/pallas_call | solution.py:464
  44.0 0.0 all-gather.4.cloned.1.call-update
  44.0 10.6 %all-to-all-done.1.gathered_ref.asked_ref = bf16[8,400,128]{2,1,0:T(8,128)(2,1)S(1)} async-done(((bf16[8,400,128]{2,1,0:T(8,128)(2,1)}), bf16[8,400,128]{2,1,0:T(8,128)(2,1)S(1)}, u32[]{:S(2)}, u32[]{:S(2)}) %all-to-all-start.1) | async-done | bytes 819232 | tf_op jit(solution)/shard_map/all_to_all | solution.py:546
  54.6 1.8 %row.1 = (bf16[144,128]{1,0:T(8,128)(2,1)S(1)}, f32[2,128,128]{2,1,0:T(8,128)S(1)}) custom-call(s32[4]{0:T(128)S(1)} %pad_add_fusion.place_ref, bf16[8,400,128]{2,1,0:T(8,128)(2,1)S(1)} %all-to-all-done.1.gathered_ref.asked_ref, bf16[16,128]{1,0:T(8,128)(2,1)S(1)} %get-tuple-element.14.gates_ref), custom_call_target="tpu_custom_call" | custom-call | flops 100000000 | bytes 1048576 | tf_op jit(solution)/shard_map/row/pallas_call | solution.py:464
  56.4 34.9 %all-gather = bf16[1152,128]{1,0:T(8,128)(2,1)S(1)} all-gather(bf16[144,128]{1,0:T(8,128)(2,1)S(1)} %get-tuple-element.15), channel_id=2, replica_groups=mesh['zh'=4,'zl'=2,'near'=8,'x'=4,'c'=2] {'zh','zl'}, dimensions={0}, use_global_device_ids=true | all-gather | bytes 331776 | tf_op jit(solution)/shard_map/all_gather | solution.py:555
  91.3 9.0 %all-gather.4.cloned.1.call-done = bf16[4096,128]{1,0:T(8,128)(2,1)} async-done(((bf16[512,128]{1,0:T(8,128)(2,1)}), bf16[4096,128]{1,0:T(8,128)(2,1)}) %all-gather.4.cloned.1.call-update) | async-done | bytes 1048592 | tf_op jit(solution)/shard_map/all_gather | solution.py:514
  100.3 1.2 copy-done.6
  101.5 3.4 %att.1 = bf16[8,272,128]{2,1,0:T(8,128)(2,1)} custom-call(s32[4]{0:T(128)S(1)} %pad_add_fusion.place_ref, bf16[8,400,128]{2,1,0:T(8,128)(2,1)S(1)} %all-to-all-done.1.gathered_ref.asked_ref, bf16[8,144,128]{2,1,0:T(8,128)(2,1)S(1)} %bitcast.13, bf16[8,512,128]{2,1,0:T(8,128)(2,1)S(1)} %bitcast.18), custom_call_target="tpu_custom_call" | custom-call | flops 2147483648 | bytes 4194304 | tf_op jit(solution)/shard_map/att/pallas_call | solution.py:464
  105.0 3.7 %all-to-all-start.2 = ((bf16[8,272,128]{2,1,0:T(8,128)(2,1)}), bf16[8,272,128]{2,1,0:T(8,128)(2,1)S(1)}, u32[]{:S(2)}, u32[]{:S(2)}) async-start(bf16[8,272,128]{2,1,0:T(8,128)(2,1)} %att.1), calls=%async_computation.2 | async-start | bytes 1114112 | tf_op jit(solution)/shard_map/all_to_all | solution.py:572
  108.7 0.0 copy-done.14
  108.7 0.6 copy-done.19
  109.3 1.2 mix.1.lin_ref
  110.6 0.0 copy-start.5
  110.6 5.4 %all-to-all-done.2.parts_ref = bf16[8,272,128]{2,1,0:T(8,128)(2,1)S(1)} async-done(((bf16[8,272,128]{2,1,0:T(8,128)(2,1)}), bf16[8,272,128]{2,1,0:T(8,128)(2,1)S(1)}, u32[]{:S(2)}, u32[]{:S(2)}) %all-to-all-start.2) | async-done | bytes 557088 | tf_op jit(solution)/shard_map/all_to_all | solution.py:572
  115.9 0.0 copy-done.5
  116.0 2.1 %out.1 = (bf16[4,256,256]{2,1,0:T(8,128)(2,1)S(1)}, bf16[4,256,256]{2,1,0:T(8,128)(2,1)S(1)}) custom-call(s32[4]{0:T(128)S(1)} %pad_add_fusion.place_ref, bf16[8,272,128]{2,1,0:T(8,128)(2,1)S(1)} %all-to-all-done.2.parts_ref, bf16[256,128]{1,0:T(8,128)(2,1)S(1)} %mix.1.lin_ref, f32[1,128]{1,0:T(1,128)S(1)} %bitcast.17, bf16[128,2048]{1,0:T(8,128)(2,1)S(1)} %copy-done.2, ...), custom_call_target="tpu_custom_call" | custom-call | flops 268435456 | bytes 2097152 | tf_op jit(solution)/shard_map/out/pallas_call | solution.py:464
  118.0 6.6 %collective-permute-start.1 = (bf16[4,256,256]{2,1,0:T(8,128)(2,1)S(1)}, bf16[4,256,256]{2,1,0:T(8,128)(2,1)S(1)}, u32[]{:S(2)}, u32[]{:S(2)}) collective-permute-start(bf16[4,256,256]{2,1,0:T(8,128)(2,1)S(1)} %get-tuple-element.20), channel_id=1, source_target_pairs={{0,1},{1,0},{2,3},{3,2},{4,5},{5,4},{6,7},{7,6},{8,9},{9,8},{10,11... | collective-permute-start | bytes 1572872 | tf_op jit(solution)/shard_map/ppermute | solution.py:450
  124.6 1.5 %collective-permute-done.1 = bf16[4,256,256]{2,1,0:T(8,128)(2,1)S(1)} collective-permute-done((bf16[4,256,256]{2,1,0:T(8,128)(2,1)S(1)}, bf16[4,256,256]{2,1,0:T(8,128)(2,1)S(1)}, u32[]{:S(2)}, u32[]{:S(2)}) %collective-permute-start.1) | collective-permute-done | bytes 524320 | tf_op jit(solution)/shard_map/ppermute | solution.py:450
  126.1 0.1 add_convert_fusion
  126.3 13.3 %all_to_all.21 = bf16[4,256,256]{2,1,0:T(8,128)(2,1)S(1)} all-to-all(bf16[4,256,256]{2,1,0:T(8,128)(2,1)S(1)} %add_convert_fusion), channel_id=1, replica_groups=mesh['zh'=4,'zl'=2,'near'=8,'x'=4,'c'=2] {'x'}, dimensions={0} | all-to-all | bytes 1048576 | tf_op jit(solution)/shard_map/all_to_all | solution.py:579
  139.6 0.7 reduce_sum.12
  (16 shorter events, 0.0 us)
Async XLA Ops:
  6.6 0.9 copy-start.12
  7.5 21.7 %copy-start.9 = (bf16[2048,128]{1,0:T(8,128)(2,1)S(1)}, bf16[2048,128]{1,0:T(8,128)(2,1)}, u32[]{:S(2)}) copy-start(bf16[2048,128]{1,0:T(8,128)(2,1)} %wv_ref.2) | copy-start | bytes 1572868
  7.5 21.7 %copy-start.10 = (bf16[2048,128]{1,0:T(8,128)(2,1)S(1)}, bf16[2048,128]{1,0:T(8,128)(2,1)}, u32[]{:S(2)}) copy-start(bf16[2048,128]{1,0:T(8,128)(2,1)} %wq_ref.1) | copy-start | bytes 1572868
  7.5 21.7 %copy-start.11 = (bf16[2048,64]{0,1:T(8,128)(2,1)S(1)}, bf16[2048,64]{0,1:T(8,128)(2,1)}, u32[]{:S(2)}) copy-start(bf16[2048,64]{0,1:T(8,128)(2,1)} %param.24) | copy-start | bytes 786436
  7.5 21.7 %copy-start.13 = (f32[256,128]{1,0:T(8,128)S(1)}, f32[256,128]{1,0:T(8,128)}, u32[]{:S(2)}) copy-start(f32[256,128]{1,0:T(8,128)} %shift_ref.1) | copy-start | bytes 393220
  7.5 21.7 %copy-start.15 = (bf16[64,128]{1,0:T(8,128)(2,1)S(1)}, bf16[64,128]{1,0:T(8,128)(2,1)}, u32[]{:S(2)}) copy-start(bf16[64,128]{1,0:T(8,128)(2,1)} %up_ref.1) | copy-start | bytes 49156
  7.5 21.7 %copy-start.17 = (f32[128]{0:T(128)S(1)}, f32[128]{0:T(128)}, u32[]{:S(2)}) copy-start(f32[128]{0:T(128)} %param.26) | copy-start | bytes 1540
  7.6 21.7 %copy-start.18 = (f32[128]{0:T(128)S(1)}, f32[128]{0:T(128)}, u32[]{:S(2)}) copy-start(f32[128]{0:T(128)} %param.28) | copy-start | bytes 1540
  8.1 21.1 %copy-start.7 = (bf16[2048,128]{1,0:T(8,128)(2,1)S(1)}, bf16[2048,128]{1,0:T(8,128)(2,1)}, u32[]{:S(2)}) copy-start(bf16[2048,128]{1,0:T(8,128)(2,1)} %wr_ref.1) | copy-start | bytes 1572868
  8.2 21.1 %copy-start.8 = (bf16[2048,128]{1,0:T(8,128)(2,1)S(1)}, bf16[2048,128]{1,0:T(8,128)(2,1)}, u32[]{:S(2)}) copy-start(bf16[2048,128]{1,0:T(8,128)(2,1)} %wk_ref.2) | copy-start | bytes 1572868
  19.9 9.4 %copy-start.4 = (f32[2048]{0:T(1024)S(1)}, f32[2048]{0:T(1024)}, u32[]{:S(2)}) copy-start(f32[2048]{0:T(1024)} %param.20) | copy-start | bytes 24580
  19.9 9.3 %collective-permute-start = (bf16[4,256,256]{2,1,0:T(8,128)(2,1)S(1)}, bf16[4,256,256]{2,1,0:T(8,128)(2,1)S(1)}, u32[]{:S(2)}, u32[]{:S(2)}) collective-permute-start(bf16[4,256,256]{2,1,0:T(8,128)(2,1)S(1)} %all_to_all.20.own_ref), channel_id=1, source_target_pairs={{0,1},{1,0},{2,3},{3,2},{4,5},{5,4},{6,7},{7,6},{8,9},{9,8},{10,11... | collective-permute-start | bytes 1572872 | tf_op jit(solution)/shard_map/ppermute | solution.py:450
  29.2 0.7 copy-start.16
  38.5 3.7 %copy-start = (bf16[2048,128]{1,0:T(8,128)(2,1)S(1)}, bf16[2048,128]{1,0:T(8,128)(2,1)}, u32[]{:S(2)}) copy-start(bf16[2048,128]{1,0:T(8,128)(2,1)} %wk_ref.3) | copy-start | bytes 1572868
  38.5 3.8 %copy-start.1 = (bf16[2048,128]{1,0:T(8,128)(2,1)S(1)}, bf16[2048,128]{1,0:T(8,128)(2,1)}, u32[]{:S(2)}) copy-start(bf16[2048,128]{1,0:T(8,128)(2,1)} %wv_ref.3) | copy-start | bytes 1572868
  38.5 16.0 %all-to-all-start.1 = ((bf16[8,400,128]{2,1,0:T(8,128)(2,1)}), bf16[8,400,128]{2,1,0:T(8,128)(2,1)S(1)}, u32[]{:S(2)}, u32[]{:S(2)}) async-start(bf16[8,400,128]{2,1,0:T(8,128)(2,1)} %get-tuple-element.13), calls=%async_computation.1 | async-start | bytes 1638400 | tf_op jit(solution)/shard_map/all_to_all | solution.py:546
  42.2 58.1 %all-gather.4.cloned.1.call-start = ((), (), s32[]{:S(2)}) async-start(), calls=%async_computation.4 | async-start | bytes 1179648 | tf_op jit(solution)/shard_map/all_gather | solution.py:514
  100.3 1.2 copy-start.6
  105.0 3.7 %copy-start.14 = (f32[2,64,64]{2,1,0:T(8,128)S(1)}, f32[2,64,64]{2,1,0:T(8,128)}, u32[]{:S(2)}) copy-start(f32[2,64,64]{2,1,0:T(8,128)} %state_ref.1) | copy-start | bytes 98308
  105.0 11.0 %all-to-all-start.2 = ((bf16[8,272,128]{2,1,0:T(8,128)(2,1)}), bf16[8,272,128]{2,1,0:T(8,128)(2,1)S(1)}, u32[]{:S(2)}, u32[]{:S(2)}) async-start(bf16[8,272,128]{2,1,0:T(8,128)(2,1)} %att.1), calls=%async_computation.2 | async-start | bytes 1114112 | tf_op jit(solution)/shard_map/all_to_all | solution.py:572
  108.7 0.7 copy-start.19
  109.3 6.6 %copy-start.2 = (bf16[128,2048]{1,0:T(8,128)(2,1)S(1)}, bf16[128,2048]{1,0:T(8,128)(2,1)}, u32[]{:S(2)}) copy-start(bf16[128,2048]{1,0:T(8,128)(2,1)} %wl_ref.1) | copy-start | bytes 1572868
  109.3 6.6 %copy-start.3 = (bf16[128,2048]{1,0:T(8,128)(2,1)S(1)}, bf16[128,2048]{1,0:T(8,128)(2,1)}, u32[]{:S(2)}) copy-start(bf16[128,2048]{1,0:T(8,128)(2,1)} %wa_ref.1) | copy-start | bytes 1572868
  110.6 5.4 %copy-start.5 = (f32[128]{0:T(128)S(1)}, f32[128]{0:T(128)}, u32[]{:S(2)}) copy-start(f32[128]{0:T(128)} %param.35) | copy-start | bytes 1540
  118.0 8.1 %collective-permute-start.1 = (bf16[4,256,256]{2,1,0:T(8,128)(2,1)S(1)}, bf16[4,256,256]{2,1,0:T(8,128)(2,1)S(1)}, u32[]{:S(2)}, u32[]{:S(2)}) collective-permute-start(bf16[4,256,256]{2,1,0:T(8,128)(2,1)S(1)} %get-tuple-element.20), channel_id=1, source_target_pairs={{0,1},{1,0},{2,3},{3,2},{4,5},{5,4},{6,7},{7,6},{8,9},{9,8},{10,11... | collective-permute-start | bytes 1572872 | tf_op jit(solution)/shard_map/ppermute | solution.py:450
Sparse Core Ops, SparseCore 0:
  45.1 55.1 all-gather.3
where the time goes:
time: 148 us; the launch traced here: 147 us
  blocking collectives  59.8 us (40%)
  waiting for transfers between devices  28 us (19%)
  starting transfers between devices  21.8 us (15%)
  Pallas kernels  19.4 us (13%)
  between operations  13.6 us (9%)
  local copies, waits for them, and re-layouts  3.44 us (2%)
    all_gather x1, blocking collectives, body(): held = lax.all_gather(row_send, KEYS)  34.9 us
    pallas_call x7, Pallas kernels, run(): pl.pallas_call(kernel, name=name, out_shape=shapes, in_specs=[smem()] + [...  19.4 us
    ppermute x2, starting transfers between devices, to_partner(): return lax.ppermute(a, axis, [(0, 1), (1, 0)])  14.4 us
    all_to_all x1, blocking collectives, body(): tiles = lax.all_to_all(pair, 'x', 0, 0, tiled=True)  13.3 us
    all_to_all x1, blocking collectives, body(): own = lax.all_to_all(copies, 'x', 0, 0, tiled=True)  11.7 us
    all_to_all x1, waiting for transfers between devices, body(): asked = lax.all_to_all(send, 'near', 0, 0, tiled=True)  10.6 us
    all_gather x1, waiting for transfers between devices, body(): keys = lax.all_gather(kv, KEYS)  9.04 us
    all_to_all x1, waiting for transfers between devices, body(): parts = lax.all_to_all(found, 'near', 0, 0, tiled=True)  5.36 us
  transfers between devices with their start and end apart: 5, of which 5 were waited for; matrix products, arithmetic and copies ran while one was open for 0% of the time, Pallas kernels for 3%

commit v1 on v0

--- a/solution.py
+++ b/solution.py
@@ -66,18 +66,26 @@
     return jnp.where(left, first, second)
 
 
+def scaled_part(ref, gain_ref, core):
+    shards, rows, depth = ref.shape
+    scaled, squares = [], jnp.zeros((rows, depth), F32)
+    for j in range(shards):
+        start = pl.multiple_of((2 * j + core) * depth, depth)
+        wide = ref[j].astype(F32)
+        scaled.append(((wide * gain_ref[:, pl.ds(start, depth)]).astype(BF16), start))
+        squares = squares + wide * wide
+    return scaled, jnp.sum(squares, axis=1, keepdims=True)
+
+
+def inverse_rms(squares, gain_ref):
+    return lax.rsqrt(squares / gain_ref.shape[1] + 1e-6)
+
+
 def scaled_pieces(place_ref, own_ref, other_ref, gain_ref):
-    shards, rows, depth = own_ref.shape
     core = place_ref[3]
-    scaled, squares = [], jnp.zeros((rows, depth), F32)
-    for c, ref in enumerate((own_ref, other_ref)):
-        for j in range(shards):
-            start = pl.multiple_of((2 * j + (core if c == 0 else 1 - core)) * depth, depth)
-            wide = ref[j].astype(F32)
-            scaled.append(((wide * gain_ref[:, pl.ds(start, depth)]).astype(BF16), start))
-            squares = squares + wide * wide
-    mean = jnp.sum(squares, axis=1, keepdims=True) / (2 * shards * depth)
-    return scaled, lax.rsqrt(mean + 1e-6)
+    own, own_squares = scaled_part(own_ref, gain_ref, core)
+    other, other_squares = scaled_part(other_ref, gain_ref, 1 - core)
+    return own + other, inverse_rms(own_squares + other_squares, gain_ref)
 
 
 def projected(scaled, inverse, *w_refs):
@@ -88,16 +96,23 @@
     return total * inverse
 
 
-def spread_kernel(place_ref, tokens_ref, out_ref):
-    tokens = tokens_ref[...]
-    for j in range(out_ref.shape[0]):
-        out_ref[j] = tokens
-
-
-def kv_kernel(place_ref, own_ref, other_ref, gain_ref, wk_ref, wv_ref, out_ref):
-    scaled, inverse = scaled_pieces(place_ref, own_ref, other_ref, gain_ref)
-    rows = own_ref.shape[1]
-    both = projected(scaled, inverse, wk_ref, wv_ref).astype(BF16)
+def place_kernel(place_ref, out_ref):
+    for i in range(out_ref.shape[0]):
+        out_ref[i] = place_ref[i]
+
+
+def kv_part_kernel(place_ref, own_ref, gain_ref, wk_ref, wv_ref, part_ref, squares_ref):
+    scaled, squares = scaled_part(own_ref, gain_ref, place_ref[3])
+    part_ref[...] = projected(scaled, 1.0, wk_ref, wv_ref)
+    squares_ref[...] = jnp.broadcast_to(squares, squares_ref.shape)
+
+
+def kv_kernel(place_ref, other_ref, gain_ref, wk_ref, wv_ref, part_ref, squares_ref, out_ref):
+    scaled, squares = scaled_part(other_ref, gain_ref, 1 - place_ref[3])
+    rows = other_ref.shape[1]
+    inverse = inverse_rms(squares + squares_ref[:, 0:1], gain_ref)
+    both = projected(scaled, 1.0, wk_ref, wv_ref) + part_ref[...]
+    both = (both * inverse).astype(BF16)
     out_ref[0:rows] = both[:, :HEAD_ATT]
     out_ref[rows:] = both[:, HEAD_ATT:]
 
@@ -373,8 +388,8 @@
             sum_ref[j] = sum_ref[j] + new
 
     def score_many(i, carry):
-        for k in range(3):
-            score(3 * i + k, False)
+        for k in range(5):
+            score(5 * i + k, False)
         return carry
 
     def score_one(k, carry):
@@ -382,24 +397,24 @@
         return carry
 
     def gather_many(i, carry):
-        gather(*(4 * i + k for k in range(4)))
+        gather(*(8 * i + k for k in range(8)))
         return carry
 
     def gather_one(k, carry):
         gather(k)
         return carry
 
-    many = z // 3
+    many = z // 5
     lax.fori_loop(0, many, score_many, 0)
-    lax.fori_loop(3 * many, z, score_one, 0)
+    lax.fori_loop(5 * many, z, score_one, 0)
     score(z, True)
     for j in range(count):
         best = jnp.max(best_ref[j], axis=1, keepdims=True)
         best = jnp.where(best > 0.5 * NEG, best, 0.0)
         best_ref[j] = jnp.broadcast_to(best, best_ref.shape[1:])
-    many = (z + 1) // 4
+    many = (z + 1) // 8
     lax.fori_loop(0, many, gather_many, 0)
-    lax.fori_loop(4 * many, z + 1, gather_one, 0)
+    lax.fori_loop(8 * many, z + 1, gather_one, 0)
     eye = iota((WIDE, WIDE), 0) == iota((WIDE, WIDE), 1)
     for j in range(count):
         total = sum_ref[j, :, HEAD_ATT:]
@@ -414,9 +429,20 @@
         out_ref[j, rows:] = in_thirds(jnp.concatenate(level, axis=0))
 
 
-def out_kernel(place_ref, parts_ref, lin_ref, gain_ref, wl_ref, wa_ref, own_ref, other_ref):
+def to_output(lin, att, wl_ref, wa_ref, core, out_ref):
+    width = out_ref.shape[2]
+    for j in range(out_ref.shape[0]):
+        start = pl.multiple_of((2 * j + core) * width, width)
+        mine = pl.ds(start, width)
+        out_ref[j] = (dot(lin, wl_ref[:, mine]) + dot(att, wa_ref[:, mine])).astype(BF16)
+
+
+def own_kernel(place_ref, att_ref, lin_ref, wl_ref, wa_ref, own_ref):
+    to_output(lin_ref[...], att_ref[...], wl_ref, wa_ref, place_ref[3], own_ref)
+
+
+def out_kernel(place_ref, parts_ref, lin_ref, gain_ref, wl_ref, wa_ref, other_ref, att_ref):
     count, rows = parts_ref.shape[0], lin_ref.shape[0]
-    core = place_ref[3]
     levels = [joined(parts_ref[j, rows:]) for j in range(count)]
     top = functools.reduce(jnp.maximum, levels)
     shares = [jnp.exp2(level - top) for level in levels]
@@ -437,13 +463,8 @@
     raw = jnp.concatenate(raw, axis=0)
     size = jnp.mean(raw * raw, axis=1, keepdims=True)
     att = (raw * lax.rsqrt(size + 1e-6) * gain_ref[...]).astype(BF16)
-    lin = lin_ref[...]
-    width = own_ref.shape[2]
-    for c, ref in enumerate((own_ref, other_ref)):
-        for j in range(ref.shape[0]):
-            start = pl.multiple_of((2 * j + (core if c == 0 else 1 - core)) * width, width)
-            mine = pl.ds(start, width)
-            ref[j] = (dot(lin, wl_ref[:, mine]) + dot(att, wa_ref[:, mine])).astype(BF16)
+    att_ref[...] = att
+    to_output(lin_ref[...], att, wl_ref, wa_ref, 1 - place_ref[3], other_ref)
 
 
 def to_partner(a, axis):
@@ -503,14 +524,29 @@
     place = jnp.stack([lax.axis_index(axis) for axis in SP + ("c",)]).astype(jnp.int32)
     gain = norm_gain.reshape(1, -1)
 
-    copies = call(spread_kernel, "spread", shape((nx, *tokens.shape), BF16), 10**10, 1 << 24, 4)(
-        place, tokens
+    place = pl.pallas_call(
+        place_kernel,
+        name="place",
+        out_shape=shape(place.shape, jnp.int32),
+        in_specs=[smem()],
+        out_specs=smem(),
+        cost_estimate=cost(10**10, 1 << 24),
+    )(place)
+    place, tokens = lax.optimization_barrier((place, tokens))
+    own = lax.all_gather(tokens, "x")
+    other = to_partner(own, "c")
+    half = rows * model_width * 256
+    part, squares = call(
+        kv_part_kernel,
+        "part",
+        (shape((rows, 256), F32), shape((rows, WIDE), F32)),
+        half,
+        1 << 21,
+        12,
+    )(place, own, gain, att_key_weight, att_value_weight)
+    kv = call(kv_kernel, "kv", shape((2 * rows, WIDE), BF16), half, 1 << 21, 12)(
+        place, other, gain, att_key_weight, att_value_weight, part, squares
     )
-    own = lax.all_to_all(copies, "x", 0, 0, tiled=True)
-    other = to_partner(own, "c")
-    kv = call(
-        kv_kernel, "kv", shape((2 * rows, WIDE), BF16), 2 * rows * model_width * 256, 1 << 21, 12
-    )(place, own, other, gain, att_key_weight, att_value_weight)
     keys = lax.all_gather(kv, KEYS)
 
     extra = 16
@@ -556,6 +592,7 @@
     lin_mixed = call(mix_kernel, "mix", shape((rows, WIDE), BF16), 10**9, 1 << 20, 12)(
         place, initial_state, held, before, reach, local, group_gain.reshape(1, -1)
     )
+    asked, lin_mixed = lax.optimization_barrier((asked, lin_mixed))
     found = call(
         functools.partial(att_kernel, rows=rows),
         "att",
@@ -572,10 +609,19 @@
     parts = lax.all_to_all(found, "near", 0, 0, tiled=True)
     width = model_width // (2 * nx)
     tile = shape((nx, rows, width), BF16)
-    mine, theirs = call(
-        out_kernel, "out", (tile, tile), 2 * rows * 256 * model_width, 1 << 21, 12
+    theirs, att = call(
+        out_kernel,
+        "out",
+        (tile, shape((rows, WIDE), BF16)),
+        rows * 256 * model_width,
+        1 << 21,
+        12,
     )(place, parts, lin_mixed, att_gain.reshape(1, -1), out_lin_weight, out_att_weight)
-    pair = (mine.astype(F32) + to_partner(theirs, "c").astype(F32)).astype(BF16)
+    theirs = to_partner(theirs, "c")
+    mine = call(own_kernel, "own", tile, rows * 256 * model_width, 1 << 21, 12)(
+        place, att, lin_mixed, out_lin_weight, out_att_weight
+    )
+    pair = (mine.astype(F32) + theirs.astype(F32)).astype(BF16)
     tiles = lax.all_to_all(pair, "x", 0, 0, tiled=True)
     return jnp.sum(tiles.astype(F32), axis=0).astype(BF16)
 
@@ -583,7 +629,7 @@
 def solution(mesh):
     sp, tp = mesh.shape["sp"], mesh.shape["tp"]
     cores = 2
-    near = math.isqrt(sp) if sp > 16 else 2
+    near = math.isqrt(sp) // 2 if sp > 16 else 2
     torus = Mesh(mesh.devices.reshape(sp // (2 * near), 2, near, tp // cores, cores), SP + TP)
     return jax.shard_map(
         body,

time: 148 us -> 148 us (level)
  waiting for transfers between devices: 28 us -> 6.83 us
  blocking collectives: 59.8 us -> 77.9 us
  local copies, waits for them, and re-layouts: 3.44 us -> 6.36 us
    all_to_all x2 -> x0, waiting for transfers between devices: 15.9 us -> none  [the longest x1 10.6 us: body(): asked = lax.all_to_all(send, 'near', 0, 0, tiled=True)]
    all_gather x0 -> x1, blocking collectives: none -> 11.2 us  [body(): own = lax.all_gather(tokens, 'x')]
    ppermute x2, starting transfers between devices: 14.4 us -> 23 us  [to_partner(): return lax.ppermute(a, axis, [(0, 1), (1, 0)])]
    all_to_all x1 -> x2, blocking collectives: 11.7 us -> 19.6 us  [the longest x1 10.3 us: body(): asked = lax.all_to_all(send, 'near', 0, 0, tiled=True)]
    all_to_all x2 -> x0, starting transfers between devices: 7.4 us -> none  [the longest x1 3.72 us: body(): parts = lax.all_to_all(found, 'near', 0, 0, tiled=True)]
    unnamed x40 -> x44, local copies, waits for them, and re-layouts: 3.44 us -> 6.36 us
    all_gather x1, waiting for transfers between devices: 9.04 us -> 6.27 us  [body(): keys = lax.all_gather(kv, KEYS)]
    pallas_call x7 -> x8, Pallas kernels: 19.4 us -> 16.7 us  [run(): pl.pallas_call(kernel, name=name, out_shape=shapes, in_specs=[smem()] + [...]
  transfers between devices with their start and end apart: 5 -> 3, of which waited for: 5 -> 2; matrix products, arithmetic and copies ran while one was open for 0% -> 0% of each run, Pallas kernels for 3% -> 8%
where the time goes in v1:
time: 148 us; the launch traced here: 147 us
  blocking collectives  77.9 us (53%)
  starting transfers between devices  23 us (16%)
  Pallas kernels  18 us (12%)
  between operations  13.6 us (9%)
  waiting for transfers between devices  6.83 us (5%)
  local copies, waits for them, and re-layouts  6.36 us (4%)
  other arithmetic  1.55 us (1%)
    all_gather x1, blocking collectives, body(): held = lax.all_gather(row_send, KEYS)  33.9 us
    ppermute x2, starting transfers between devices, to_partner(): return lax.ppermute(a, axis, [(0, 1), (1, 0)])  23 us
    pallas_call x8, Pallas kernels, run(): pl.pallas_call(kernel, name=name, out_shape=shapes, in_specs=[smem()] + [...  16.7 us
    all_to_all x1, blocking collectives, body(): tiles = lax.all_to_all(pair, 'x', 0, 0, tiled=True)  13.2 us
    all_gather x1, blocking collectives, body(): own = lax.all_gather(tokens, 'x')  11.2 us
    all_to_all x1, blocking collectives, body(): asked = lax.all_to_all(send, 'near', 0, 0, tiled=True)  10.3 us
    all_to_all x1, blocking collectives, body(): parts = lax.all_to_all(found, 'near', 0, 0, tiled=True)  9.25 us
    unnamed x44, local copies, waits for them, and re-layouts  6.36 us
  transfers between devices with their start and end apart: 3, of which 2 were waited for; matrix products, arithmetic and copies ran while one was open for 0% of the time, Pallas kernels for 8%

profile of v1, /device:TPU:1, one launch (start us, length us, event | category | flops | bytes accessed | tf_op | source)
XLA Modules:
  0.0 147.3 jit_solution(9735477654355665770)
XLA Ops:
  6.5 0.0 all-gather.5.cloned.1.call-start
  6.5 0.7 pad_add_fusion.place_ref
  7.2 0.0 copy-start.10
  7.2 0.0 copy-start.13
  7.2 1.3 place.1.place_ref
  8.6 0.0 copy-done.21
  8.6 0.0 copy-start.6
  8.6 0.0 copy-start.9
  8.6 0.0 copy-start.14
  8.6 0.0 copy-start.17
  8.6 11.2 %all-gather = bf16[1024,256]{1,0:T(8,128)(2,1)S(1)} all-gather(bf16[256,256]{1,0:T(8,128)(2,1)S(1)} %copy-done.21), channel_id=2, replica_groups=mesh['zh'=8,'zl'=2,'near'=4,'x'=4,'c'=2] {'x'}, dimensions={0}, use_global_device_ids=true | all-gather | bytes 655360 | tf_op jit(solution)/shard_map/all_gather | solution.py:536
  19.8 10.5 %collective-permute-start = (bf16[4,256,256]{2,1,0:T(8,128)(2,1)S(1)}, bf16[4,256,256]{2,1,0:T(8,128)(2,1)S(1)}, u32[]{:S(2)}, u32[]{:S(2)}) collective-permute-start(bf16[4,256,256]{2,1,0:T(8,128)(2,1)S(1)} %bitcast.14), channel_id=1, source_target_pairs={{0,1},{1,0},{2,3},{3,2},{4,5},{5,4},{6,7},{7,6},{8,9},{9,8},{10,11... | collective-permute-start | bytes 1572872 | tf_op jit(solution)/shard_map/ppermute | solution.py:471
  30.3 0.0 copy-done
  30.3 0.0 copy-done.1
  30.3 0.0 copy-done.4
  30.3 0.0 copy-start.5
  30.3 0.6 copy-done.5
  30.9 0.9 part.1
  31.8 0.0 collective-permute-done.other_ref
  31.8 1.6 %kv.1 = bf16[512,128]{1,0:T(8,128)(2,1)} custom-call(s32[4]{0:T(128)S(1)} %copy-done.5, bf16[4,256,256]{2,1,0:T(8,128)(2,1)S(1)} %collective-permute-done.other_ref, f32[1,2048]{1,0:T(1,128)S(1)} %bitcast.20, bf16[2048,128]{1,0:T(8,128)(2,1)S(1)} %copy-done, bf16[2048,128]{1,0:T(8,128)(2,1)S(1)} %copy-done.1, f32[256,256]{1,0:T(8,128)S(1)} %get-tuple-element.28.part_ref, ...), custom_call_target="tpu_custom_call" | custom-call | flops 134217728 | bytes 2097152 | tf_op jit(solution)/shard_map/kv/pallas_call | solution.py:485
  33.4 0.0 all-gather.5.cloned.1.call-update
  33.4 0.0 copy-done.10
  33.4 0.0 copy-done.13
  33.5 0.0 copy-done.6
  33.5 0.0 copy-done.9
  33.5 0.0 copy-start.11
  33.5 1.0 copy-done.11
  34.5 1.0 copy-done.12
  35.6 0.7 copy-done.16
  36.3 0.7 copy-done.18
  37.0 0.7 copy-done.19
  37.6 7.8 %lin.1 = (bf16[4,400,128]{2,1,0:T(8,128)(2,1)S(1)}, bf16[16,128]{1,0:T(8,128)(2,1)S(1)}, f32[256,128]{1,0:T(8,128)S(1)}, f32[256,128]{1,0:T(8,128)S(1)}) custom-call(s32[4]{0:T(128)S(1)} %copy-done.6, bf16[4,256,256]{2,1,0:T(8,128)(2,1)S(1)} %bitcast.16, bf16[4,256,256]{2,1,0:T(8,128)(2,1)S(1)} %collective-permute-done.other_ref, f32[1,2048]{1,0:T(1,128)S(1)} %bitcast.21, ...), custom_call_target="tpu_custom_call" | custom-call | flops 4000000000 | bytes 4194304 | tf_op jit(solution)/shard_map/lin/pallas_call | solution.py:485
  45.4 10.3 %all_to_all.15.gathered_ref.asked_ref = bf16[4,400,128]{2,1,0:T(8,128)(2,1)S(1)} all-to-all(bf16[4,400,128]{2,1,0:T(8,128)(2,1)S(1)} %get-tuple-element.21), channel_id=1, replica_groups=mesh['zh'=8,'zl'=2,'near'=4,'x'=4,'c'=2] {'near'}, dimensions={0} | all-to-all | bytes 819200 | tf_op jit(solution)/shard_map/all_to_all | solution.py:582
  55.7 1.1 row.1
  56.9 33.9 %all-gather.1 = bf16[2304,128]{1,0:T(8,128)(2,1)S(1)} all-gather(bf16[144,128]{1,0:T(8,128)(2,1)S(1)} %get-tuple-element.23), channel_id=3, replica_groups=mesh['zh'=8,'zl'=2,'near'=4,'x'=4,'c'=2] {'zh','zl'}, dimensions={0}, use_global_device_ids=true | all-gather | bytes 626688 | tf_op jit(solution)/shard_map/all_gather | solution.py:591
  90.8 1.2 mix.1.lin_ref
  92.0 6.3 %all-gather.5.cloned.1.call-done = bf16[8192,128]{1,0:T(8,128)(2,1)} async-done(((bf16[512,128]{1,0:T(8,128)(2,1)}), bf16[8192,128]{1,0:T(8,128)(2,1)}) %all-gather.5.cloned.1.call-update) | async-done | bytes 2097168 | tf_op jit(solution)/shard_map/all_gather | solution.py:550
  98.3 1.6 %copy-done.8 = bf16[8192,128]{1,0:T(8,128)(2,1)S(1)} copy-done((bf16[8192,128]{1,0:T(8,128)(2,1)S(1)}, bf16[8192,128]{1,0:T(8,128)(2,1)}, u32[]{:S(2)}) %copy-start.8) | copy-done | bytes 2097176
  99.9 1.7 %att.1 = bf16[4,272,128]{2,1,0:T(8,128)(2,1)S(1)} custom-call(s32[4]{0:T(128)S(1)} %copy-done.6, bf16[4,400,128]{2,1,0:T(8,128)(2,1)S(1)} %all_to_all.15.gathered_ref.asked_ref, bf16[16,144,128]{2,1,0:T(8,128)(2,1)S(1)} %bitcast.18, bf16[16,512,128]{2,1,0:T(8,128)(2,1)S(1)} %bitcast.23), custom_call_target="tpu_custom_call" | custom-call | flops 2147483648 | bytes 4194304 | tf_op jit(solution)/shard_map/att/pallas_call | solution.py:485
  101.5 9.2 %all_to_all.16.parts_ref = bf16[4,272,128]{2,1,0:T(8,128)(2,1)S(1)} all-to-all(bf16[4,272,128]{2,1,0:T(8,128)(2,1)S(1)} %att.1), channel_id=1, replica_groups=mesh['zh'=8,'zl'=2,'near'=4,'x'=4,'c'=2] {'near'}, dimensions={0} | all-to-all | bytes 557056 | tf_op jit(solution)/shard_map/all_to_all | solution.py:609
  110.8 0.0 copy-done.7
  110.8 1.5 %out.1 = (bf16[4,256,256]{2,1,0:T(8,128)(2,1)S(1)}, bf16[256,128]{1,0:T(8,128)(2,1)S(1)}) custom-call(s32[4]{0:T(128)S(1)} %copy-done.6, bf16[4,272,128]{2,1,0:T(8,128)(2,1)S(1)} %all_to_all.16.parts_ref, bf16[256,128]{1,0:T(8,128)(2,1)S(1)} %mix.1.lin_ref, f32[1,128]{1,0:T(1,128)S(1)} %bitcast.22, bf16[128,2048]{1,0:T(8,128)(2,1)S(1)} %copy-done.2, ...), custom_call_target="tpu_custom_call" | custom-call | flops 134217728 | bytes 2097152 | tf_op jit(solution)/shard_map/out/pallas_call | solution.py:485
  112.3 12.6 %collective-permute-start.1 = (bf16[4,256,256]{2,1,0:T(8,128)(2,1)S(1)}, bf16[4,256,256]{2,1,0:T(8,128)(2,1)S(1)}, u32[]{:S(2)}, u32[]{:S(2)}) collective-permute-start(bf16[4,256,256]{2,1,0:T(8,128)(2,1)S(1)} %get-tuple-element.32), channel_id=1, source_target_pairs={{0,1},{1,0},{2,3},{3,2},{4,5},{5,4},{6,7},{7,6},{8,9},{9,8},{10,11... | collective-permute-start | bytes 1572872 | tf_op jit(solution)/shard_map/ppermute | solution.py:471
  124.9 1.0 own.1
  125.9 0.5 collective-permute-done.1
  126.4 0.1 add_convert_fusion
  126.5 13.2 %all_to_all.17 = bf16[4,256,256]{2,1,0:T(8,128)(2,1)S(1)} all-to-all(bf16[4,256,256]{2,1,0:T(8,128)(2,1)S(1)} %add_convert_fusion), channel_id=1, replica_groups=mesh['zh'=8,'zl'=2,'near'=4,'x'=4,'c'=2] {'x'}, dimensions={0} | all-to-all | bytes 1048576 | tf_op jit(solution)/shard_map/all_to_all | solution.py:625
  139.7 0.7 reduce_sum.12
  (20 shorter events, 0.0 us)
Async XLA Ops:
  6.5 91.7 %all-gather.5.cloned.1.call-start = ((), (), s32[]{:S(2)}) async-start(), calls=%async_computation.3 | async-start | bytes 2228224 | tf_op jit(solution)/shard_map/all_gather | solution.py:550
  7.2 1.4 copy-start.21
  7.2 23.1 %copy-start = (bf16[2048,128]{1,0:T(8,128)(2,1)S(1)}, bf16[2048,128]{1,0:T(8,128)(2,1)}, u32[]{:S(2)}) copy-start(bf16[2048,128]{1,0:T(8,128)(2,1)} %wk_ref.5) | copy-start | bytes 1572868
  7.2 23.1 %copy-start.1 = (bf16[2048,128]{1,0:T(8,128)(2,1)S(1)}, bf16[2048,128]{1,0:T(8,128)(2,1)}, u32[]{:S(2)}) copy-start(bf16[2048,128]{1,0:T(8,128)(2,1)} %wv_ref.5) | copy-start | bytes 1572868
  7.2 23.1 %copy-start.4 = (f32[2048]{0:T(1024)S(1)}, f32[2048]{0:T(1024)}, u32[]{:S(2)}) copy-start(f32[2048]{0:T(1024)} %param.20) | copy-start | bytes 24580
  7.2 26.2 %copy-start.10 = (bf16[2048,128]{1,0:T(8,128)(2,1)S(1)}, bf16[2048,128]{1,0:T(8,128)(2,1)}, u32[]{:S(2)}) copy-start(bf16[2048,128]{1,0:T(8,128)(2,1)} %wk_ref.3) | copy-start | bytes 1572868
  7.2 26.2 %copy-start.13 = (bf16[2048,64]{0,1:T(8,128)(2,1)S(1)}, bf16[2048,64]{0,1:T(8,128)(2,1)}, u32[]{:S(2)}) copy-start(bf16[2048,64]{0,1:T(8,128)(2,1)} %param.24) | copy-start | bytes 786436
  8.6 24.9 %copy-start.6 = (s32[4]{0:T(128)S(1)}, s32[4]{0:T(128)}, u32[]{:S(2)}) copy-start(s32[4]{0:T(128)} %place.1.place_ref) | copy-start | bytes 52
  8.6 24.9 %copy-start.9 = (bf16[2048,128]{1,0:T(8,128)(2,1)S(1)}, bf16[2048,128]{1,0:T(8,128)(2,1)}, u32[]{:S(2)}) copy-start(bf16[2048,128]{1,0:T(8,128)(2,1)} %wr_ref.1) | copy-start | bytes 1572868
  8.6 24.9 %copy-start.14 = (f32[256,128]{1,0:T(8,128)S(1)}, f32[256,128]{1,0:T(8,128)}, u32[]{:S(2)}) copy-start(f32[256,128]{1,0:T(8,128)} %shift_ref.1) | copy-start | bytes 393220
  8.6 24.9 %copy-start.17 = (f32[256,1]{0,1:T(1,128)S(1)}, f32[256,1]{0,1:T(1,128)}, u32[]{:S(2)}) copy-start(f32[256,1]{0,1:T(1,128)} %param.34) | copy-start | bytes 3076
  19.8 12.0 %collective-permute-start = (bf16[4,256,256]{2,1,0:T(8,128)(2,1)S(1)}, bf16[4,256,256]{2,1,0:T(8,128)(2,1)S(1)}, u32[]{:S(2)}, u32[]{:S(2)}) collective-permute-start(bf16[4,256,256]{2,1,0:T(8,128)(2,1)S(1)} %bitcast.14), channel_id=1, source_target_pairs={{0,1},{1,0},{2,3},{3,2},{4,5},{5,4},{6,7},{7,6},{8,9},{9,8},{10,11... | collective-permute-start | bytes 1572872 | tf_op jit(solution)/shard_map/ppermute | solution.py:471
  30.3 0.6 copy-start.5
  33.5 1.0 copy-start.11
  34.5 1.0 copy-start.12
  35.6 0.7 copy-start.16
  36.3 0.7 copy-start.18
  37.0 0.7 copy-start.19
  37.6 53.2 %copy-start.15 = (f32[2,64,64]{2,1,0:T(8,128)S(1)}, f32[2,64,64]{2,1,0:T(8,128)}, u32[]{:S(2)}) copy-start(f32[2,64,64]{2,1,0:T(8,128)} %state_ref.1) | copy-start | bytes 98308
  37.6 53.2 %copy-start.20 = (f32[128]{0:T(128)S(1)}, f32[128]{0:T(128)}, u32[]{:S(2)}) copy-start(f32[128]{0:T(128)} %param.29) | copy-start | bytes 1540
  98.3 1.6 %copy-start.8 = (bf16[8192,128]{1,0:T(8,128)(2,1)S(1)}, bf16[8192,128]{1,0:T(8,128)(2,1)}, u32[]{:S(2)}) copy-start(bf16[8192,128]{1,0:T(8,128)(2,1)} %all-gather.5.cloned.1.call-done) | copy-start | bytes 6291460
  99.9 10.9 %copy-start.2 = (bf16[128,2048]{1,0:T(8,128)(2,1)S(1)}, bf16[128,2048]{1,0:T(8,128)(2,1)}, u32[]{:S(2)}) copy-start(bf16[128,2048]{1,0:T(8,128)(2,1)} %wl_ref.3) | copy-start | bytes 1572868
  99.9 10.9 %copy-start.3 = (bf16[128,2048]{1,0:T(8,128)(2,1)S(1)}, bf16[128,2048]{1,0:T(8,128)(2,1)}, u32[]{:S(2)}) copy-start(bf16[128,2048]{1,0:T(8,128)(2,1)} %wa_ref.3) | copy-start | bytes 1572868
  99.9 10.9 %copy-start.7 = (f32[128]{0:T(128)S(1)}, f32[128]{0:T(128)}, u32[]{:S(2)}) copy-start(f32[128]{0:T(128)} %param.35) | copy-start | bytes 1540
  112.3 14.1 %collective-permute-start.1 = (bf16[4,256,256]{2,1,0:T(8,128)(2,1)S(1)}, bf16[4,256,256]{2,1,0:T(8,128)(2,1)S(1)}, u32[]{:S(2)}, u32[]{:S(2)}) collective-permute-start(bf16[4,256,256]{2,1,0:T(8,128)(2,1)S(1)} %get-tuple-element.32), channel_id=1, source_target_pairs={{0,1},{1,0},{2,3},{3,2},{4,5},{5,4},{6,7},{7,6},{8,9},{9,8},{10,11... | collective-permute-start | bytes 1572872 | tf_op jit(solution)/shard_map/ppermute | solution.py:471
Sparse Core Ops, SparseCore 0:
  33.6 64.6 all-gather.4

commit v2 on v0

--- a/solution.py
+++ b/solution.py
@@ -130,6 +130,63 @@
     return ahead, after
 
 
+def head_lanes(rows):
+    lane = iota((rows, WIDE), 1)
+    return [lane < HEAD_LIN, lane >= HEAD_LIN]
+
+
+def below(h, half):
+    tall = iota((half, half), 0)
+    flat = iota((half, half), 1)
+    level = h.bit_length()
+    near = (tall >> level) == (flat >> level)
+    return near & ((tall & h) != 0) & ((flat & h) == 0)
+
+
+def fill_pairs(pairs_ref, asking, now, key, rate, ahead, after, step):
+    rows = asking.shape[0]
+    half = rows // 2
+    row = iota((rows, WIDE), 0)
+    heads = head_lanes(rows)
+    eye = iota((half, half), 0) == iota((half, half), 1)
+    blocks = slice(0, half), slice(half, rows)
+    for m, source in enumerate((key, rate)):
+        same = by_head(asking * source) if now else None
+        for n in range(2):
+            for b in range(2):
+                cols = slice(m * rows + b * half, m * rows + (b + 1) * half)
+                start = jnp.zeros((half, half), F32)
+                if now:
+                    column = same[blocks[b], n * HEAD_LIN : n * HEAD_LIN + 1]
+                    start = jnp.where(eye, column, 0.0)
+                pairs_ref[n, blocks[b], cols] = start
+            cols = slice(m * rows + half, (m + 1) * rows)
+            pairs_ref[n, blocks[0], cols] = jnp.zeros((half, half), F32)
+    h = 1
+    while h < rows:
+        late = (row & h) != 0
+        reach = ahead[h] if step is None else ahead[h] + step
+        left = asking * jnp.where(late, jnp.exp(reach), 0.0)
+        left = [jnp.where(mine, left, 0.0).astype(BF16) for mine in heads]
+        from_s = jnp.where(late, 0.0, jnp.exp(after[h]))
+        right = (key * from_s).astype(BF16), (rate * from_s).astype(BF16)
+        for b in range(2) if h < half else (1,):
+            c = b if h < half else 0
+            product = dot(
+                jnp.concatenate([a[blocks[b]] for a in left], axis=0),
+                jnp.concatenate([a[blocks[c]] for a in right], axis=0),
+                ((1,), (1,)),
+            )
+            for n in range(2):
+                for m in range(2):
+                    cols = slice(m * rows + c * half, m * rows + (c + 1) * half)
+                    new = product[n * half : (n + 1) * half, m * half : (m + 1) * half]
+                    if h < half:
+                        new = jnp.where(below(h, half), new, pairs_ref[n, blocks[b], cols])
+                    pairs_ref[n, blocks[b], cols] = new
+        h *= 2
+
+
 def lin_kernel(
     place_ref,
     own_ref,
@@ -147,8 +204,8 @@
     gate_ref,
     send_ref,
     gates_ref,
-    reach_ref,
-    local_ref,
+    rows_ref,
+    value_ref,
     pairs_ref,
 ):
     scaled, inverse = scaled_pieces(place_ref, own_ref, other_ref, gain_ref)
@@ -169,69 +226,19 @@
 
     ahead, after = spans(log_decay)
     half = rows // 2
-    lane = iota((rows, WIDE), 1)
-    row = iota((rows, WIDE), 0)
-    tall = iota((half, half), 0)
-    flat = iota((half, half), 1)
-    heads = [lane < HEAD_LIN, lane >= HEAD_LIN]
-    eye = tall == flat
+    heads = head_lanes(rows)
     blocks = slice(0, half), slice(half, rows)
-
-    def of_heads(a):
-        return [jnp.where(mine, a, 0.0).astype(BF16) for mine in heads]
-
-    def below(h):
-        level = h.bit_length()
-        near = (tall >> level) == (flat >> level)
-        return near & ((tall & h) != 0) & ((flat & h) == 0)
-
-    for m, source in enumerate((key, rate)):
-        now = by_head(recv * source)
-        for n in range(2):
-            for b in range(2):
-                cols = slice(m * rows + b * half, m * rows + (b + 1) * half)
-                same_row = now[blocks[b], n * HEAD_LIN : n * HEAD_LIN + 1]
-                pairs_ref[n, 1, blocks[b], cols] = jnp.where(eye, same_row, 0.0)
-                pairs_ref[n, 0, blocks[b], cols] = jnp.zeros((half, half), F32)
-            cols = slice(m * rows + half, (m + 1) * rows)
-            for k in range(2):
-                pairs_ref[n, k, blocks[0], cols] = jnp.zeros((half, half), F32)
-    h = 1
-    while h < rows:
-        late = (row & h) != 0
-        to_u = jnp.where(late, jnp.exp(ahead[h]), 0.0)
-        to_q = jnp.where(late, jnp.exp(ahead[h] + log_decay), 0.0)
-        from_s = jnp.where(late, 0.0, jnp.exp(after[h]))
-        right = (key * from_s).astype(BF16), (rate * from_s).astype(BF16)
-        left = of_heads(unit * to_u) + of_heads(recv * to_q)
-        for b in range(2) if h < half else (1,):
-            c = b if h < half else 0
-            product = dot(
-                jnp.concatenate([a[blocks[b]] for a in left], axis=0),
-                jnp.concatenate([a[blocks[c]] for a in right], axis=0),
-                ((1,), (1,)),
-            )
-            for k in range(2):
-                for n in range(2):
-                    for m in range(2):
-                        cols = slice(m * rows + c * half, m * rows + (c + 1) * half)
-                        new = product[
-                            (2 * k + n) * half : (2 * k + n + 1) * half,
-                            m * half : (m + 1) * half,
-                        ]
-                        if h < half:
-                            new = jnp.where(below(h), new, pairs_ref[n, k, blocks[b], cols])
-                        pairs_ref[n, k, blocks[b], cols] = new
-        h *= 2
+    eye = iota((half, half), 0) == iota((half, half), 1)
+    fill_pairs(pairs_ref, unit, None, key, rate, ahead, after, None)
 
     solved = {}
     h = 1
     while h < half:
-        here = below(h)
+        here = below(h, half)
         for n in range(2):
             for b in range(2):
                 cols = slice(rows + b * half, rows + (b + 1) * half)
-                links = jnp.where(here, pairs_ref[n, 0, blocks[b], cols], 0.0)
+                links = jnp.where(here, pairs_ref[n, blocks[b], cols], 0.0)
                 if h == 1:
                     solved[n, b] = jnp.where(eye, 1.0, 0.0) - links
                 else:
@@ -240,23 +247,21 @@
         h *= 2
 
     full_u = unit * jnp.exp(ahead[rows])
-    full_q = recv * jnp.exp(ahead[rows] + log_decay)
     tail = jnp.exp(after[rows])
     full_k = key * tail
     full_r = rate * tail
-    reach, local, moved = [], [], []
+    moved = []
     for n in range(2):
-        add = dot2(pairs_ref[n, 0, :, :rows], value)
+        add = dot2(pairs_ref[n, :, :rows], value)
         source = jnp.where(heads[n], full_u, pltpu.roll(add, HEAD_LIN, 1))
         first = dot3(solved[n, 0], source[:half])
-        later = source[half:] - dot3(pairs_ref[n, 0, half:, rows : rows + half], first)
+        later = source[half:] - dot3(pairs_ref[n, half:, rows : rows + half], first)
         along = jnp.concatenate([first, dot3(solved[n, 1], later)], axis=0)
-        taken = dot3(pairs_ref[n, 1, :, rows:], along)
-        reach.append(full_q - taken)
-        local.append(dot2(pairs_ref[n, 1, :, :rows], value) - pltpu.roll(taken, HEAD_LIN, 1))
+        rows_ref[n] = along
         moved.append(dot3(along, full_r, ((0,), (0,))))
-    reach_ref[...] = jnp.where(heads[0], reach[0], reach[1])
-    local_ref[...] = jnp.where(heads[0], local[0], local[1])
+    for i, kept in enumerate((recv, key, rate, log_decay)):
+        rows_ref[2 + i] = kept
+    value_ref[...] = value
 
     lane = iota((WIDE, WIDE), 1)
     row = iota((WIDE, WIDE), 0)
@@ -272,6 +277,23 @@
     whole = send_ref[0]
     for j in range(1, send_ref.shape[0]):
         send_ref[j] = whole
+
+
+def reach_kernel(place_ref, rows_ref, value_ref, reach_ref, local_ref, pairs_ref):
+    recv, key, rate, log_decay = (rows_ref[2 + i] for i in range(4))
+    rows = recv.shape[0]
+    ahead, after = spans(log_decay)
+    heads = head_lanes(rows)
+    fill_pairs(pairs_ref, recv, True, key, rate, ahead, after, log_decay)
+    full_q = recv * jnp.exp(ahead[rows] + log_decay)
+    value = value_ref[...]
+    reach, local = [], []
+    for n in range(2):
+        taken = dot3(pairs_ref[n, :, rows:], rows_ref[n])
+        reach.append(full_q - taken)
+        local.append(dot2(pairs_ref[n, :, :rows], value) - pltpu.roll(taken, HEAD_LIN, 1))
+    reach_ref[...] = jnp.where(heads[0], reach[0], reach[1])
+    local_ref[...] = jnp.where(heads[0], local[0], local[1])
 
 
 def unpacked(packed):
@@ -508,25 +530,20 @@
     )
     own = lax.all_to_all(copies, "x", 0, 0, tiled=True)
     other = to_partner(own, "c")
-    kv = call(
-        kv_kernel, "kv", shape((2 * rows, WIDE), BF16), 2 * rows * model_width * 256, 1 << 21, 12
-    )(place, own, other, gain, att_key_weight, att_value_weight)
-    keys = lax.all_gather(kv, KEYS)
-
     extra = 16
-    send, gates, reach, local = call(
+    send, gates, kept, value = call(
         lin_kernel,
         "lin",
         (
             shape((ny, rows + WIDE + extra, WIDE), BF16),
             shape((extra, WIDE), BF16),
-            shape((rows, WIDE), F32),
-            shape((rows, WIDE), F32),
+            shape((6, rows, WIDE), F32),
+            shape((rows, WIDE), BF16),
         ),
         4 * 10**9,
         1 << 22,
         24,
-        scratch=[pltpu.VMEM((2, 2, rows, 2 * rows), F32)],
+        scratch=[pltpu.VMEM((2, rows, 2 * rows), F32)],
     )(
         place,
         own,
@@ -543,7 +560,22 @@
         learn_rate.reshape(1, -1),
         gate_cache.reshape(rows // WIDE, WIDE),
     )
+    send, own, other = lax.optimization_barrier((send, own, other))
     asked = lax.all_to_all(send, "near", 0, 0, tiled=True)
+    kv = call(
+        kv_kernel, "kv", shape((2 * rows, WIDE), BF16), 2 * rows * model_width * 256, 1 << 21, 12
+    )(place, own, other, gain, att_key_weight, att_value_weight)
+    kv, kept = lax.optimization_barrier((kv, kept))
+    keys = lax.all_gather(kv, KEYS)
+    reach, local = call(
+        reach_kernel,
+        "reach",
+        (shape((rows, WIDE), F32), shape((rows, WIDE), F32)),
+        2 * 10**9,
+        1 << 21,
+        16,
+        scratch=[pltpu.VMEM((2, rows, 2 * rows), F32)],
+    )(place, kept, value)
     row_send, before = call(
         functools.partial(row_kernel, rows=rows),
         "row",
@@ -556,6 +588,7 @@
     lin_mixed = call(mix_kernel, "mix", shape((rows, WIDE), BF16), 10**9, 1 << 20, 12)(
         place, initial_state, held, before, reach, local, group_gain.reshape(1, -1)
     )
+    asked, lin_mixed = lax.optimization_barrier((asked, lin_mixed))
     found = call(
         functools.partial(att_kernel, rows=rows),
         "att",

time: 148 us -> 148 us (level)
  blocking collectives: 59.8 us -> 68.9 us
  waiting for transfers between devices: 28 us -> 18.9 us
  starting transfers between devices: 21.8 us -> 18.5 us
  local copies, waits for them, and re-layouts: 3.44 us -> 6.13 us
    all_to_all x0 -> x1, blocking collectives: none -> 12.4 us  [body(): parts = lax.all_to_all(found, 'near', 0, 0, tiled=True)]
    all_to_all x1 -> x0, waiting for transfers between devices: 5.36 us -> none  [body(): parts = lax.all_to_all(found, 'near', 0, 0, tiled=True)]
    all_to_all x1 -> x0, starting transfers between devices: 3.72 us -> none  [body(): parts = lax.all_to_all(found, 'near', 0, 0, tiled=True)]
    all_to_all x1, waiting for transfers between devices: 10.6 us -> 7.2 us  [body(): asked = lax.all_to_all(send, 'near', 0, 0, tiled=True)]
    unnamed x40 -> x44, local copies, waits for them, and re-layouts: 3.44 us -> 6.13 us
    all_gather x1, blocking collectives: 34.9 us -> 33.1 us  [body(): held = lax.all_gather(row_send, KEYS)]
    all_to_all x1, blocking collectives: 13.3 us -> 11.6 us  [body(): tiles = lax.all_to_all(pair, 'x', 0, 0, tiled=True)]
    pallas_call x7 -> x8, Pallas kernels: 19.4 us -> 20.2 us  [run(): pl.pallas_call(kernel, name=name, out_shape=shapes, in_specs=[smem()] + [...]
  transfers between devices with their start and end apart: 5 -> 4, of which waited for: 5 -> 4; matrix products, arithmetic and copies ran while one was open for 0% -> 0% of each run, Pallas kernels for 3% -> 5%
where the time goes in v2:
time: 148 us; the launch traced here: 147 us
  blocking collectives  68.9 us (47%)
  Pallas kernels  20.2 us (14%)
  waiting for transfers between devices  18.9 us (13%)
  starting transfers between devices  18.5 us (12%)
  between operations  13.6 us (9%)
  local copies, waits for them, and re-layouts  6.13 us (4%)
    all_gather x1, blocking collectives, body(): held = lax.all_gather(row_send, KEYS)  33.1 us
    pallas_call x8, Pallas kernels, run(): pl.pallas_call(kernel, name=name, out_shape=shapes, in_specs=[smem()] + [...  20.2 us
    ppermute x2, starting transfers between devices, to_partner(): return lax.ppermute(a, axis, [(0, 1), (1, 0)])  14.8 us
    all_to_all x1, blocking collectives, body(): parts = lax.all_to_all(found, 'near', 0, 0, tiled=True)  12.4 us
    all_to_all x1, blocking collectives, body(): own = lax.all_to_all(copies, 'x', 0, 0, tiled=True)  11.7 us
    all_to_all x1, blocking collectives, body(): tiles = lax.all_to_all(pair, 'x', 0, 0, tiled=True)  11.6 us
    all_gather x1, waiting for transfers between devices, body(): keys = lax.all_gather(kv, KEYS)  8.69 us
    all_to_all x1, waiting for transfers between devices, body(): asked = lax.all_to_all(send, 'near', 0, 0, tiled=True)  7.2 us
  transfers between devices with their start and end apart: 4, of which 4 were waited for; matrix products, arithmetic and copies ran while one was open for 0% of the time, Pallas kernels for 5%

profile of v2, /device:TPU:1, one launch (start us, length us, event | category | flops | bytes accessed | tf_op | source)
XLA Modules:
  0.0 147.3 jit_solution(13623265283479038522)
XLA Ops:
  6.5 0.1 pad_add_fusion.place_ref
  6.6 0.9 copy-done.12
  7.5 0.0 copy-start.15
  7.5 0.0 copy-start.17
  7.6 0.0 copy-start.18
  7.6 0.6 spread.1
  8.1 0.0 copy-start.7
  8.2 0.0 copy-start.8
  8.2 11.7 %all_to_all.20.own_ref = bf16[4,256,256]{2,1,0:T(8,128)(2,1)S(1)} all-to-all(bf16[4,256,256]{2,1,0:T(8,128)(2,1)S(1)} %spread.1), channel_id=1, replica_groups=mesh['zh'=4,'zl'=2,'near'=8,'x'=4,'c'=2] {'x'}, dimensions={0} | all-to-all | bytes 1048576 | tf_op jit(solution)/shard_map/all_to_all | solution.py:531
  19.9 7.8 %collective-permute-start = (bf16[4,256,256]{2,1,0:T(8,128)(2,1)S(1)}, bf16[4,256,256]{2,1,0:T(8,128)(2,1)S(1)}, u32[]{:S(2)}, u32[]{:S(2)}) collective-permute-start(bf16[4,256,256]{2,1,0:T(8,128)(2,1)S(1)} %all_to_all.20.own_ref), channel_id=1, source_target_pairs={{0,1},{1,0},{2,3},{3,2},{4,5},{5,4},{6,7},{7,6},{8,9},{9,8},{10,11... | collective-permute-start | bytes 1572872 | tf_op jit(solution)/shard_map/ppermute | solution.py:472
  27.7 1.5 %collective-permute-done.other_ref = bf16[4,256,256]{2,1,0:T(8,128)(2,1)S(1)} collective-permute-done((bf16[4,256,256]{2,1,0:T(8,128)(2,1)S(1)}, bf16[4,256,256]{2,1,0:T(8,128)(2,1)S(1)}, u32[]{:S(2)}, u32[]{:S(2)}) %collective-permute-start) | collective-permute-done | bytes 524320 | tf_op jit(solution)/shard_map/ppermute | solution.py:472
  29.2 0.0 copy-done.9
  29.2 0.0 copy-done.10
  29.2 0.0 copy-done.11
  29.2 0.0 copy-done.13
  29.2 0.0 copy-done.15
  29.2 0.0 copy-done.17
  29.2 0.0 copy-done.18
  29.2 0.0 copy-done.7
  29.2 0.0 copy-done.8
  29.3 0.6 copy-done.16
  29.9 8.1 %lin.1 = (bf16[8,400,128]{2,1,0:T(8,128)(2,1)}, bf16[16,128]{1,0:T(8,128)(2,1)S(1)}, f32[6,256,128]{2,1,0:T(8,128)S(1)}, bf16[256,128]{1,0:T(8,128)(2,1)S(1)}) custom-call(s32[4]{0:T(128)S(1)} %pad_add_fusion.place_ref, bf16[4,256,256]{2,1,0:T(8,128)(2,1)S(1)} %all_to_all.20.own_ref, bf16[4,256,256]{2,1,0:T(8,128)(2,1)S(1)} %collective-permute-done.other_ref, ...), custom_call_target="tpu_custom_call" | custom-call | flops 4000000000 | bytes 4194304 | tf_op jit(solution)/shard_map/lin/pallas_call | solution.py:486
  37.9 0.9 copy-done.20
  38.8 3.7 %all-to-all-start.1 = ((bf16[8,400,128]{2,1,0:T(8,128)(2,1)}), bf16[8,400,128]{2,1,0:T(8,128)(2,1)S(1)}, u32[]{:S(2)}, u32[]{:S(2)}) async-start(bf16[8,400,128]{2,1,0:T(8,128)(2,1)} %get-tuple-element.23), calls=%async_computation.1 | async-start | bytes 1638400 | tf_op jit(solution)/shard_map/all_to_all | solution.py:564
  42.5 0.0 all-gather.4.cloned.1.call-start
  42.6 1.7 %kv.1 = bf16[512,128]{1,0:T(8,128)(2,1)} custom-call(s32[4]{0:T(128)S(1)} %pad_add_fusion.place_ref, bf16[4,256,256]{2,1,0:T(8,128)(2,1)S(1)} %all_to_all.20.own_ref, bf16[4,256,256]{2,1,0:T(8,128)(2,1)S(1)} %collective-permute-done.other_ref, f32[1,2048]{1,0:T(1,128)S(1)} %bitcast.16, bf16[2048,128]{1,0:T(8,128)(2,1)S(1)} %copy-done, ...), custom_call_target="tpu_custom_call" | custom-call | flops 268435456 | bytes 2097152 | tf_op jit(solution)/shard_map/kv/pallas_call | solution.py:486
  44.3 0.0 all-gather.4.cloned.1.call-update
  44.3 1.1 copy-done.21
  45.4 2.2 %reach.1 = (f32[256,128]{1,0:T(8,128)S(1)}, f32[256,128]{1,0:T(8,128)S(1)}) custom-call(s32[4]{0:T(128)S(1)} %pad_add_fusion.place_ref, f32[6,256,128]{2,1,0:T(8,128)S(1)} %copy-done.21, bf16[256,128]{1,0:T(8,128)(2,1)S(1)} %get-tuple-element.31.value_ref), custom_call_target="tpu_custom_call" | custom-call | flops 2000000000 | bytes 2097152 | tf_op jit(solution)/shard_map/reach/pallas_call | solution.py:486
  47.6 7.2 %all-to-all-done.1.gathered_ref.asked_ref = bf16[8,400,128]{2,1,0:T(8,128)(2,1)S(1)} async-done(((bf16[8,400,128]{2,1,0:T(8,128)(2,1)}), bf16[8,400,128]{2,1,0:T(8,128)(2,1)S(1)}, u32[]{:S(2)}, u32[]{:S(2)}) %all-to-all-start.1) | async-done | bytes 819232 | tf_op jit(solution)/shard_map/all_to_all | solution.py:564
  54.9 1.8 %row.1 = (bf16[144,128]{1,0:T(8,128)(2,1)S(1)}, f32[2,128,128]{2,1,0:T(8,128)S(1)}) custom-call(s32[4]{0:T(128)S(1)} %pad_add_fusion.place_ref, bf16[8,400,128]{2,1,0:T(8,128)(2,1)S(1)} %all-to-all-done.1.gathered_ref.asked_ref, bf16[16,128]{1,0:T(8,128)(2,1)S(1)} %get-tuple-element.24.gates_ref), custom_call_target="tpu_custom_call" | custom-call | flops 100000000 | bytes 1048576 | tf_op jit(solution)/shard_map/row/pallas_call | solution.py:486
  56.7 0.0 copy-start.14
  56.7 33.1 %all-gather = bf16[1152,128]{1,0:T(8,128)(2,1)S(1)} all-gather(bf16[144,128]{1,0:T(8,128)(2,1)S(1)} %get-tuple-element.25), channel_id=2, replica_groups=mesh['zh'=4,'zl'=2,'near'=8,'x'=4,'c'=2] {'zh','zl'}, dimensions={0}, use_global_device_ids=true | all-gather | bytes 331776 | tf_op jit(solution)/shard_map/all_gather | solution.py:587
  89.8 0.7 copy-done.19
  90.5 1.2 mix.1.lin_ref
  91.7 8.7 %all-gather.4.cloned.1.call-done = bf16[4096,128]{1,0:T(8,128)(2,1)} async-done(((bf16[512,128]{1,0:T(8,128)(2,1)}), bf16[4096,128]{1,0:T(8,128)(2,1)}) %all-gather.4.cloned.1.call-update) | async-done | bytes 1048592 | tf_op jit(solution)/shard_map/all_gather | solution.py:569
  100.4 1.2 copy-done.6
  101.6 2.6 %att.1 = bf16[8,272,128]{2,1,0:T(8,128)(2,1)S(1)} custom-call(s32[4]{0:T(128)S(1)} %pad_add_fusion.place_ref, bf16[8,400,128]{2,1,0:T(8,128)(2,1)S(1)} %all-to-all-done.1.gathered_ref.asked_ref, bf16[8,144,128]{2,1,0:T(8,128)(2,1)S(1)} %bitcast.14, bf16[8,512,128]{2,1,0:T(8,128)(2,1)S(1)} %bitcast.18), custom_call_target="tpu_custom_call" | custom-call | flops 2147483648 | bytes 4194304 | tf_op jit(solution)/shard_map/att/pallas_call | solution.py:486
  104.2 0.0 copy-start.2
  104.2 0.0 copy-start.3
  104.2 12.4 %all_to_all.21.parts_ref = bf16[8,272,128]{2,1,0:T(8,128)(2,1)S(1)} all-to-all(bf16[8,272,128]{2,1,0:T(8,128)(2,1)S(1)} %att.1), channel_id=1, replica_groups=mesh['zh'=4,'zl'=2,'near'=8,'x'=4,'c'=2] {'near'}, dimensions={0} | all-to-all | bytes 1114112 | tf_op jit(solution)/shard_map/all_to_all | solution.py:605
  116.7 0.6 copy-done.5
  117.3 2.1 %out.1 = (bf16[4,256,256]{2,1,0:T(8,128)(2,1)S(1)}, bf16[4,256,256]{2,1,0:T(8,128)(2,1)S(1)}) custom-call(s32[4]{0:T(128)S(1)} %pad_add_fusion.place_ref, bf16[8,272,128]{2,1,0:T(8,128)(2,1)S(1)} %all_to_all.21.parts_ref, bf16[256,128]{1,0:T(8,128)(2,1)S(1)} %mix.1.lin_ref, f32[1,128]{1,0:T(1,128)S(1)} %bitcast.17, bf16[128,2048]{1,0:T(8,128)(2,1)S(1)} %copy-done.2, ...), custom_call_target="tpu_custom_call" | custom-call | flops 268435456 | bytes 2097152 | tf_op jit(solution)/shard_map/out/pallas_call | solution.py:486
  119.4 7.0 %collective-permute-start.1 = (bf16[4,256,256]{2,1,0:T(8,128)(2,1)S(1)}, bf16[4,256,256]{2,1,0:T(8,128)(2,1)S(1)}, u32[]{:S(2)}, u32[]{:S(2)}) collective-permute-start(bf16[4,256,256]{2,1,0:T(8,128)(2,1)S(1)} %get-tuple-element.38), channel_id=1, source_target_pairs={{0,1},{1,0},{2,3},{3,2},{4,5},{5,4},{6,7},{7,6},{8,9},{9,8},{10,11... | collective-permute-start | bytes 1572872 | tf_op jit(solution)/shard_map/ppermute | solution.py:472
  126.4 1.5 %collective-permute-done.1 = bf16[4,256,256]{2,1,0:T(8,128)(2,1)S(1)} collective-permute-done((bf16[4,256,256]{2,1,0:T(8,128)(2,1)S(1)}, bf16[4,256,256]{2,1,0:T(8,128)(2,1)S(1)}, u32[]{:S(2)}, u32[]{:S(2)}) %collective-permute-start.1) | collective-permute-done | bytes 524320 | tf_op jit(solution)/shard_map/ppermute | solution.py:472
  127.9 0.1 add_convert_fusion
  128.1 11.6 %all_to_all.22 = bf16[4,256,256]{2,1,0:T(8,128)(2,1)S(1)} all-to-all(bf16[4,256,256]{2,1,0:T(8,128)(2,1)S(1)} %add_convert_fusion), channel_id=1, replica_groups=mesh['zh'=4,'zl'=2,'near'=8,'x'=4,'c'=2] {'x'}, dimensions={0} | all-to-all | bytes 1048576 | tf_op jit(solution)/shard_map/all_to_all | solution.py:612
  139.7 0.7 reduce_sum.12
  (20 shorter events, 0.0 us)
Async XLA Ops:
  6.6 0.9 copy-start.12
  7.5 21.7 %copy-start.9 = (bf16[2048,128]{1,0:T(8,128)(2,1)S(1)}, bf16[2048,128]{1,0:T(8,128)(2,1)}, u32[]{:S(2)}) copy-start(bf16[2048,128]{1,0:T(8,128)(2,1)} %wv_ref.2) | copy-start | bytes 1572868
  7.5 21.7 %copy-start.10 = (bf16[2048,128]{1,0:T(8,128)(2,1)S(1)}, bf16[2048,128]{1,0:T(8,128)(2,1)}, u32[]{:S(2)}) copy-start(bf16[2048,128]{1,0:T(8,128)(2,1)} %wq_ref.1) | copy-start | bytes 1572868
  7.5 21.7 %copy-start.11 = (bf16[2048,64]{0,1:T(8,128)(2,1)S(1)}, bf16[2048,64]{0,1:T(8,128)(2,1)}, u32[]{:S(2)}) copy-start(bf16[2048,64]{0,1:T(8,128)(2,1)} %param.24) | copy-start | bytes 786436
  7.5 21.7 %copy-start.13 = (f32[256,128]{1,0:T(8,128)S(1)}, f32[256,128]{1,0:T(8,128)}, u32[]{:S(2)}) copy-start(f32[256,128]{1,0:T(8,128)} %shift_ref.1) | copy-start | bytes 393220
  7.5 21.7 %copy-start.15 = (bf16[64,128]{1,0:T(8,128)(2,1)S(1)}, bf16[64,128]{1,0:T(8,128)(2,1)}, u32[]{:S(2)}) copy-start(bf16[64,128]{1,0:T(8,128)(2,1)} %up_ref.1) | copy-start | bytes 49156
  7.5 21.7 %copy-start.17 = (f32[128]{0:T(128)S(1)}, f32[128]{0:T(128)}, u32[]{:S(2)}) copy-start(f32[128]{0:T(128)} %param.26) | copy-start | bytes 1540
  7.6 21.7 %copy-start.18 = (f32[128]{0:T(128)S(1)}, f32[128]{0:T(128)}, u32[]{:S(2)}) copy-start(f32[128]{0:T(128)} %param.28) | copy-start | bytes 1540
  8.1 21.1 %copy-start.7 = (bf16[2048,128]{1,0:T(8,128)(2,1)S(1)}, bf16[2048,128]{1,0:T(8,128)(2,1)}, u32[]{:S(2)}) copy-start(bf16[2048,128]{1,0:T(8,128)(2,1)} %wr_ref.1) | copy-start | bytes 1572868
  8.2 21.1 %copy-start.8 = (bf16[2048,128]{1,0:T(8,128)(2,1)S(1)}, bf16[2048,128]{1,0:T(8,128)(2,1)}, u32[]{:S(2)}) copy-start(bf16[2048,128]{1,0:T(8,128)(2,1)} %wk_ref.2) | copy-start | bytes 1572868
  19.9 9.4 %copy-start.4 = (f32[2048]{0:T(1024)S(1)}, f32[2048]{0:T(1024)}, u32[]{:S(2)}) copy-start(f32[2048]{0:T(1024)} %param.20) | copy-start | bytes 24580
  19.9 9.3 %collective-permute-start = (bf16[4,256,256]{2,1,0:T(8,128)(2,1)S(1)}, bf16[4,256,256]{2,1,0:T(8,128)(2,1)S(1)}, u32[]{:S(2)}, u32[]{:S(2)}) collective-permute-start(bf16[4,256,256]{2,1,0:T(8,128)(2,1)S(1)} %all_to_all.20.own_ref), channel_id=1, source_target_pairs={{0,1},{1,0},{2,3},{3,2},{4,5},{5,4},{6,7},{7,6},{8,9},{9,8},{10,11... | collective-permute-start | bytes 1572872 | tf_op jit(solution)/shard_map/ppermute | solution.py:472
  29.2 0.7 copy-start.16
  37.9 0.9 copy-start.20
  38.8 3.7 %copy-start = (bf16[2048,128]{1,0:T(8,128)(2,1)S(1)}, bf16[2048,128]{1,0:T(8,128)(2,1)}, u32[]{:S(2)}) copy-start(bf16[2048,128]{1,0:T(8,128)(2,1)} %wk_ref.3) | copy-start | bytes 1572868
  38.8 3.8 %copy-start.1 = (bf16[2048,128]{1,0:T(8,128)(2,1)S(1)}, bf16[2048,128]{1,0:T(8,128)(2,1)}, u32[]{:S(2)}) copy-start(bf16[2048,128]{1,0:T(8,128)(2,1)} %wv_ref.3) | copy-start | bytes 1572868
  38.8 16.0 %all-to-all-start.1 = ((bf16[8,400,128]{2,1,0:T(8,128)(2,1)}), bf16[8,400,128]{2,1,0:T(8,128)(2,1)S(1)}, u32[]{:S(2)}, u32[]{:S(2)}) async-start(bf16[8,400,128]{2,1,0:T(8,128)(2,1)} %get-tuple-element.23), calls=%async_computation.1 | async-start | bytes 1638400 | tf_op jit(solution)/shard_map/all_to_all | solution.py:564
  42.5 57.9 %all-gather.4.cloned.1.call-start = ((), (), s32[]{:S(2)}) async-start(), calls=%async_computation.4 | async-start | bytes 1179648 | tf_op jit(solution)/shard_map/all_gather | solution.py:569
  44.3 1.1 copy-start.21
  56.7 33.2 %copy-start.14 = (f32[2,64,64]{2,1,0:T(8,128)S(1)}, f32[2,64,64]{2,1,0:T(8,128)}, u32[]{:S(2)}) copy-start(f32[2,64,64]{2,1,0:T(8,128)} %state_ref.1) | copy-start | bytes 98308
  89.8 0.7 copy-start.19
  100.4 1.2 copy-start.6
  104.2 12.5 %copy-start.2 = (bf16[128,2048]{1,0:T(8,128)(2,1)S(1)}, bf16[128,2048]{1,0:T(8,128)(2,1)}, u32[]{:S(2)}) copy-start(bf16[128,2048]{1,0:T(8,128)(2,1)} %wl_ref.1) | copy-start | bytes 1572868
  104.2 12.4 %copy-start.3 = (bf16[128,2048]{1,0:T(8,128)(2,1)S(1)}, bf16[128,2048]{1,0:T(8,128)(2,1)}, u32[]{:S(2)}) copy-start(bf16[128,2048]{1,0:T(8,128)(2,1)} %wa_ref.1) | copy-start | bytes 1572868
  116.7 0.7 copy-start.5
  119.4 8.6 %collective-permute-start.1 = (bf16[4,256,256]{2,1,0:T(8,128)(2,1)S(1)}, bf16[4,256,256]{2,1,0:T(8,128)(2,1)S(1)}, u32[]{:S(2)}, u32[]{:S(2)}) collective-permute-start(bf16[4,256,256]{2,1,0:T(8,128)(2,1)S(1)} %get-tuple-element.38), channel_id=1, source_target_pairs={{0,1},{1,0},{2,3},{3,2},{4,5},{5,4},{6,7},{7,6},{8,9},{9,8},{10,11... | collective-permute-start | bytes 1572872 | tf_op jit(solution)/shard_map/ppermute | solution.py:472
Sparse Core Ops, SparseCore 0:
  45.4 54.9 all-gather.3

commit v3 on v1

--- a/solution.py
+++ b/solution.py
@@ -96,9 +96,10 @@
     return total * inverse
 
 
-def place_kernel(place_ref, out_ref):
-    for i in range(out_ref.shape[0]):
-        out_ref[i] = place_ref[i]
+def spread_kernel(place_ref, tokens_ref, out_ref):
+    tokens = tokens_ref[...]
+    for j in range(out_ref.shape[0]):
+        out_ref[j] = tokens
 
 
 def kv_part_kernel(place_ref, own_ref, gain_ref, wk_ref, wv_ref, part_ref, squares_ref):
@@ -524,16 +525,10 @@
     place = jnp.stack([lax.axis_index(axis) for axis in SP + ("c",)]).astype(jnp.int32)
     gain = norm_gain.reshape(1, -1)
 
-    place = pl.pallas_call(
-        place_kernel,
-        name="place",
-        out_shape=shape(place.shape, jnp.int32),
-        in_specs=[smem()],
-        out_specs=smem(),
-        cost_estimate=cost(10**10, 1 << 24),
-    )(place)
-    place, tokens = lax.optimization_barrier((place, tokens))
-    own = lax.all_gather(tokens, "x")
+    copies = call(spread_kernel, "spread", shape((nx, *tokens.shape), BF16), 10**10, 1 << 24, 4)(
+        place, tokens
+    )
+    own = lax.all_to_all(copies, "x", 0, 0, tiled=True)
     other = to_partner(own, "c")
     half = rows * model_width * 256
     part, squares = call(

time: 148 us -> 145 us (0.980)
  the two profiles are of different devices: /device:TPU:1 before, /device:TPU:480 now
where the time goes in v3:
time: 145 us; the launch traced here: 143 us
  blocking collectives  83.6 us (58%)
  Pallas kernels  24.6 us (17%)
  between operations  13.6 us (9%)
  waiting for transfers between devices  12.7 us (9%)
  starting transfers between devices  3.97 us (3%)
  local copies, waits for them, and re-layouts  3.47 us (2%)
    all_gather x1, blocking collectives, body(): held = lax.all_gather(row_send, KEYS)  32.8 us
    pallas_call x9, Pallas kernels, run(): pl.pallas_call(kernel, name=name, out_shape=shapes, in_specs=[smem()] + [...  24.6 us
    all_to_all x1, blocking collectives, body(): own = lax.all_to_all(copies, 'x', 0, 0, tiled=True)  13.6 us
    all_to_all x1, blocking collectives, body(): tiles = lax.all_to_all(pair, 'x', 0, 0, tiled=True)  12.9 us
    all_to_all x1, blocking collectives, body(): asked = lax.all_to_all(send, 'near', 0, 0, tiled=True)  12.8 us
    all_to_all x1, blocking collectives, body(): parts = lax.all_to_all(found, 'near', 0, 0, tiled=True)  11.5 us
    all_gather x1, waiting for transfers between devices, body(): keys = lax.all_gather(kv, KEYS)  10.8 us
    ppermute x2, starting transfers between devices, to_partner(): return lax.ppermute(a, axis, [(0, 1), (1, 0)])  3.97 us
  transfers between devices with their start and end apart: 3, of which 3 were waited for; matrix products, arithmetic and copies ran while one was open for 0% of the time, Pallas kernels for 10%

profile of v3, /device:TPU:480, one launch (start us, length us, event | category | flops | bytes accessed | tf_op | source)
XLA Modules:
  0.0 142.9 jit_solution(8405482572936595303)
XLA Ops:
  6.5 0.0 all-gather.4.cloned.1.call-start
  6.5 0.1 pad_add_fusion.place_ref
  6.6 0.9 copy-done.12
  7.5 0.6 spread.1
  8.1 13.6 %all_to_all.20.own_ref = bf16[4,256,256]{2,1,0:T(8,128)(2,1)S(1)} all-to-all(bf16[4,256,256]{2,1,0:T(8,128)(2,1)S(1)} %spread.1), channel_id=1, replica_groups=mesh['zh'=8,'zl'=2,'near'=4,'x'=4,'c'=2] {'x'}, dimensions={0} | all-to-all | bytes 1048576 | tf_op jit(solution)/shard_map/all_to_all | solution.py:531
  21.7 0.0 copy-start.11
  21.7 0.0 copy-start.15
  21.7 0.0 copy-start.16
  21.7 0.0 copy-start.17
  21.7 0.0 copy-start.18
  21.8 2.1 %collective-permute-start = (bf16[4,256,256]{2,1,0:T(8,128)(2,1)S(1)}, bf16[4,256,256]{2,1,0:T(8,128)(2,1)S(1)}, u32[]{:S(2)}, u32[]{:S(2)}) collective-permute-start(bf16[4,256,256]{2,1,0:T(8,128)(2,1)S(1)} %all_to_all.20.own_ref), channel_id=1, source_target_pairs={{0,1},{1,0},{2,3},{3,2},{4,5},{5,4},{6,7},{7,6},{8,9},{9,8},{10,11... | collective-permute-start | bytes 1572872 | tf_op jit(solution)/shard_map/ppermute | solution.py:472
  23.8 0.0 copy-done
  23.8 0.0 copy-done.1
  23.8 0.0 copy-done.4
  23.8 0.9 part.1
  24.7 1.0 collective-permute-done.other_ref
  25.7 1.6 %kv.1 = bf16[512,128]{1,0:T(8,128)(2,1)} custom-call(s32[4]{0:T(128)S(1)} %pad_add_fusion.place_ref, bf16[4,256,256]{2,1,0:T(8,128)(2,1)S(1)} %collective-permute-done.other_ref, f32[1,2048]{1,0:T(1,128)S(1)} %bitcast.16, bf16[2048,128]{1,0:T(8,128)(2,1)S(1)} %copy-done, bf16[2048,128]{1,0:T(8,128)(2,1)S(1)} %copy-done.1, ...), custom_call_target="tpu_custom_call" | custom-call | flops 134217728 | bytes 2097152 | tf_op jit(solution)/shard_map/kv/pallas_call | solution.py:486
  27.3 0.0 all-gather.4.cloned.1.call-update
  27.3 0.0 copy-done.7
  27.3 0.0 copy-done.8
  27.3 0.0 copy-done.9
  27.4 0.0 copy-done.10
  27.4 0.0 copy-done.11
  27.4 0.0 copy-done.15
  27.4 0.0 copy-done.16
  27.4 0.0 copy-done.17
  27.4 0.0 copy-done.18
  27.4 0.0 copy-start.13
  27.4 0.9 copy-done.13
  28.3 7.8 %lin.1 = (bf16[4,400,128]{2,1,0:T(8,128)(2,1)S(1)}, bf16[16,128]{1,0:T(8,128)(2,1)S(1)}, f32[256,128]{1,0:T(8,128)S(1)}, f32[256,128]{1,0:T(8,128)S(1)}) custom-call(s32[4]{0:T(128)S(1)} %pad_add_fusion.place_ref, bf16[4,256,256]{2,1,0:T(8,128)(2,1)S(1)} %all_to_all.20.own_ref, bf16[4,256,256]{2,1,0:T(8,128)(2,1)S(1)} %collective-permute-done.other_ref, ...), custom_call_target="tpu_custom_call" | custom-call | flops 4000000000 | bytes 4194304 | tf_op jit(solution)/shard_map/lin/pallas_call | solution.py:486
  36.1 12.8 %all_to_all.21.gathered_ref.asked_ref = bf16[4,400,128]{2,1,0:T(8,128)(2,1)S(1)} all-to-all(bf16[4,400,128]{2,1,0:T(8,128)(2,1)S(1)} %get-tuple-element.17), channel_id=1, replica_groups=mesh['zh'=8,'zl'=2,'near'=4,'x'=4,'c'=2] {'near'}, dimensions={0} | all-to-all | bytes 819200 | tf_op jit(solution)/shard_map/all_to_all | solution.py:577
  48.9 1.1 row.1
  50.0 32.8 %all-gather = bf16[2304,128]{1,0:T(8,128)(2,1)S(1)} all-gather(bf16[144,128]{1,0:T(8,128)(2,1)S(1)} %get-tuple-element.19), channel_id=2, replica_groups=mesh['zh'=8,'zl'=2,'near'=4,'x'=4,'c'=2] {'zh','zl'}, dimensions={0}, use_global_device_ids=true | all-gather | bytes 626688 | tf_op jit(solution)/shard_map/all_gather | solution.py:586
  82.8 0.0 copy-done.14
  82.8 0.0 copy-done.19
  82.8 3.6 %mix.1.lin_ref = bf16[256,128]{1,0:T(8,128)(2,1)S(1)} custom-call(s32[4]{0:T(128)S(1)} %pad_add_fusion.place_ref, f32[2,64,64]{2,1,0:T(8,128)S(1)} %copy-done.14, bf16[16,144,128]{2,1,0:T(8,128)(2,1)S(1)} %bitcast.13, f32[2,128,128]{2,1,0:T(8,128)S(1)} %get-tuple-element.20.before_ref, f32[256,128]{1,0:T(8,128)S(1)} %get-tuple-element.21.reach_ref, ...), custom_call_target="tpu_custom_call" | custom-call | flops 1000000000 | bytes 1048576 | tf_op jit(solution)/shard_map/mix/pallas_call | solution.py:486
  86.4 10.8 %all-gather.4.cloned.1.call-done = bf16[8192,128]{1,0:T(8,128)(2,1)} async-done(((bf16[512,128]{1,0:T(8,128)(2,1)}), bf16[8192,128]{1,0:T(8,128)(2,1)}) %all-gather.4.cloned.1.call-update) | async-done | bytes 2097168 | tf_op jit(solution)/shard_map/all_gather | solution.py:545
  97.2 1.6 %copy-done.6 = bf16[8192,128]{1,0:T(8,128)(2,1)S(1)} copy-done((bf16[8192,128]{1,0:T(8,128)(2,1)S(1)}, bf16[8192,128]{1,0:T(8,128)(2,1)}, u32[]{:S(2)}) %copy-start.6) | copy-done | bytes 2097176
  98.8 6.6 %att.1 = bf16[4,272,128]{2,1,0:T(8,128)(2,1)S(1)} custom-call(s32[4]{0:T(128)S(1)} %pad_add_fusion.place_ref, bf16[4,400,128]{2,1,0:T(8,128)(2,1)S(1)} %all_to_all.21.gathered_ref.asked_ref, bf16[16,144,128]{2,1,0:T(8,128)(2,1)S(1)} %bitcast.14, bf16[16,512,128]{2,1,0:T(8,128)(2,1)S(1)} %bitcast.19), custom_call_target="tpu_custom_call" | custom-call | flops 2147483648 | bytes 4194304 | tf_op jit(solution)/shard_map/att/pallas_call | solution.py:486
  105.4 11.5 %all_to_all.22.parts_ref = bf16[4,272,128]{2,1,0:T(8,128)(2,1)S(1)} all-to-all(bf16[4,272,128]{2,1,0:T(8,128)(2,1)S(1)} %att.1), channel_id=1, replica_groups=mesh['zh'=8,'zl'=2,'near'=4,'x'=4,'c'=2] {'near'}, dimensions={0} | all-to-all | bytes 557056 | tf_op jit(solution)/shard_map/all_to_all | solution.py:604
  116.9 0.0 copy-done.2
  116.9 1.5 %out.1 = (bf16[4,256,256]{2,1,0:T(8,128)(2,1)S(1)}, bf16[256,128]{1,0:T(8,128)(2,1)S(1)}) custom-call(s32[4]{0:T(128)S(1)} %pad_add_fusion.place_ref, bf16[4,272,128]{2,1,0:T(8,128)(2,1)S(1)} %all_to_all.22.parts_ref, bf16[256,128]{1,0:T(8,128)(2,1)S(1)} %mix.1.lin_ref, f32[1,128]{1,0:T(1,128)S(1)} %bitcast.18, bf16[128,2048]{1,0:T(8,128)(2,1)S(1)} %copy-done.2, ...), custom_call_target="tpu_custom_call" | custom-call | flops 134217728 | bytes 2097152 | tf_op jit(solution)/shard_map/out/pallas_call | solution.py:486
  118.4 1.9 %collective-permute-start.1 = (bf16[4,256,256]{2,1,0:T(8,128)(2,1)S(1)}, bf16[4,256,256]{2,1,0:T(8,128)(2,1)S(1)}, u32[]{:S(2)}, u32[]{:S(2)}) collective-permute-start(bf16[4,256,256]{2,1,0:T(8,128)(2,1)S(1)} %get-tuple-element.28), channel_id=1, source_target_pairs={{0,1},{1,0},{2,3},{3,2},{4,5},{5,4},{6,7},{7,6},{8,9},{9,8},{10,11... | collective-permute-start | bytes 1572872 | tf_op jit(solution)/shard_map/ppermute | solution.py:472
  120.4 1.0 own.1
  121.3 0.9 collective-permute-done.1
  122.2 0.1 add_convert_fusion
  122.4 12.9 %all_to_all.23 = bf16[4,256,256]{2,1,0:T(8,128)(2,1)S(1)} all-to-all(bf16[4,256,256]{2,1,0:T(8,128)(2,1)S(1)} %add_convert_fusion), channel_id=1, replica_groups=mesh['zh'=8,'zl'=2,'near'=4,'x'=4,'c'=2] {'x'}, dimensions={0} | all-to-all | bytes 1048576 | tf_op jit(solution)/shard_map/all_to_all | solution.py:620
  135.3 0.7 reduce_sum.12
  (16 shorter events, 0.0 us)
Async XLA Ops:
  6.5 90.7 %all-gather.4.cloned.1.call-start = ((), (), s32[]{:S(2)}) async-start(), calls=%async_computation.4 | async-start | bytes 2228224 | tf_op jit(solution)/shard_map/all_gather | solution.py:545
  6.6 0.9 copy-start.12
  7.5 16.3 %copy-start = (bf16[2048,128]{1,0:T(8,128)(2,1)S(1)}, bf16[2048,128]{1,0:T(8,128)(2,1)}, u32[]{:S(2)}) copy-start(bf16[2048,128]{1,0:T(8,128)(2,1)} %wk_ref.5) | copy-start | bytes 1572868
  7.5 16.3 %copy-start.1 = (bf16[2048,128]{1,0:T(8,128)(2,1)S(1)}, bf16[2048,128]{1,0:T(8,128)(2,1)}, u32[]{:S(2)}) copy-start(bf16[2048,128]{1,0:T(8,128)(2,1)} %wv_ref.5) | copy-start | bytes 1572868
  7.5 16.3 %copy-start.4 = (f32[2048]{0:T(1024)S(1)}, f32[2048]{0:T(1024)}, u32[]{:S(2)}) copy-start(f32[2048]{0:T(1024)} %param.20) | copy-start | bytes 24580
  21.7 5.6 %copy-start.7 = (bf16[2048,128]{1,0:T(8,128)(2,1)S(1)}, bf16[2048,128]{1,0:T(8,128)(2,1)}, u32[]{:S(2)}) copy-start(bf16[2048,128]{1,0:T(8,128)(2,1)} %wr_ref.1) | copy-start | bytes 1572868
  21.7 5.7 %copy-start.8 = (bf16[2048,128]{1,0:T(8,128)(2,1)S(1)}, bf16[2048,128]{1,0:T(8,128)(2,1)}, u32[]{:S(2)}) copy-start(bf16[2048,128]{1,0:T(8,128)(2,1)} %wk_ref.3) | copy-start | bytes 1572868
  21.7 5.7 %copy-start.9 = (bf16[2048,128]{1,0:T(8,128)(2,1)S(1)}, bf16[2048,128]{1,0:T(8,128)(2,1)}, u32[]{:S(2)}) copy-start(bf16[2048,128]{1,0:T(8,128)(2,1)} %wv_ref.3) | copy-start | bytes 1572868
  21.7 5.7 %copy-start.10 = (bf16[2048,128]{1,0:T(8,128)(2,1)S(1)}, bf16[2048,128]{1,0:T(8,128)(2,1)}, u32[]{:S(2)}) copy-start(bf16[2048,128]{1,0:T(8,128)(2,1)} %wq_ref.1) | copy-start | bytes 1572868
  21.7 5.7 %copy-start.11 = (bf16[2048,64]{0,1:T(8,128)(2,1)S(1)}, bf16[2048,64]{0,1:T(8,128)(2,1)}, u32[]{:S(2)}) copy-start(bf16[2048,64]{0,1:T(8,128)(2,1)} %param.24) | copy-start | bytes 786436
  21.7 5.7 %copy-start.15 = (bf16[64,128]{1,0:T(8,128)(2,1)S(1)}, bf16[64,128]{1,0:T(8,128)(2,1)}, u32[]{:S(2)}) copy-start(bf16[64,128]{1,0:T(8,128)(2,1)} %up_ref.1) | copy-start | bytes 49156
  21.7 5.7 %copy-start.16 = (f32[256,1]{0,1:T(1,128)S(1)}, f32[256,1]{0,1:T(1,128)}, u32[]{:S(2)}) copy-start(f32[256,1]{0,1:T(1,128)} %param.34) | copy-start | bytes 3076
  21.7 5.7 %copy-start.17 = (f32[128]{0:T(128)S(1)}, f32[128]{0:T(128)}, u32[]{:S(2)}) copy-start(f32[128]{0:T(128)} %param.26) | copy-start | bytes 1540
  21.7 5.7 %copy-start.18 = (f32[128]{0:T(128)S(1)}, f32[128]{0:T(128)}, u32[]{:S(2)}) copy-start(f32[128]{0:T(128)} %param.28) | copy-start | bytes 1540
  21.8 3.9 %collective-permute-start = (bf16[4,256,256]{2,1,0:T(8,128)(2,1)S(1)}, bf16[4,256,256]{2,1,0:T(8,128)(2,1)S(1)}, u32[]{:S(2)}, u32[]{:S(2)}) collective-permute-start(bf16[4,256,256]{2,1,0:T(8,128)(2,1)S(1)} %all_to_all.20.own_ref), channel_id=1, source_target_pairs={{0,1},{1,0},{2,3},{3,2},{4,5},{5,4},{6,7},{7,6},{8,9},{9,8},{10,11... | collective-permute-start | bytes 1572872 | tf_op jit(solution)/shard_map/ppermute | solution.py:472
  27.4 0.9 copy-start.13
  28.3 54.5 %copy-start.14 = (f32[2,64,64]{2,1,0:T(8,128)S(1)}, f32[2,64,64]{2,1,0:T(8,128)}, u32[]{:S(2)}) copy-start(f32[2,64,64]{2,1,0:T(8,128)} %state_ref.1) | copy-start | bytes 98308
  28.3 54.5 %copy-start.19 = (f32[128]{0:T(128)S(1)}, f32[128]{0:T(128)}, u32[]{:S(2)}) copy-start(f32[128]{0:T(128)} %param.29) | copy-start | bytes 1540
  97.2 1.6 %copy-start.6 = (bf16[8192,128]{1,0:T(8,128)(2,1)S(1)}, bf16[8192,128]{1,0:T(8,128)(2,1)}, u32[]{:S(2)}) copy-start(bf16[8192,128]{1,0:T(8,128)(2,1)} %all-gather.4.cloned.1.call-done) | copy-start | bytes 6291460
  98.8 18.1 %copy-start.2 = (bf16[128,2048]{1,0:T(8,128)(2,1)S(1)}, bf16[128,2048]{1,0:T(8,128)(2,1)}, u32[]{:S(2)}) copy-start(bf16[128,2048]{1,0:T(8,128)(2,1)} %wl_ref.3) | copy-start | bytes 1572868
  98.8 18.1 %copy-start.3 = (bf16[128,2048]{1,0:T(8,128)(2,1)S(1)}, bf16[128,2048]{1,0:T(8,128)(2,1)}, u32[]{:S(2)}) copy-start(bf16[128,2048]{1,0:T(8,128)(2,1)} %wa_ref.3) | copy-start | bytes 1572868
  98.8 18.1 %copy-start.5 = (f32[128]{0:T(128)S(1)}, f32[128]{0:T(128)}, u32[]{:S(2)}) copy-start(f32[128]{0:T(128)} %param.35) | copy-start | bytes 1540
  118.4 3.8 %collective-permute-start.1 = (bf16[4,256,256]{2,1,0:T(8,128)(2,1)S(1)}, bf16[4,256,256]{2,1,0:T(8,128)(2,1)S(1)}, u32[]{:S(2)}, u32[]{:S(2)}) collective-permute-start(bf16[4,256,256]{2,1,0:T(8,128)(2,1)S(1)} %get-tuple-element.28), channel_id=1, source_target_pairs={{0,1},{1,0},{2,3},{3,2},{4,5},{5,4},{6,7},{7,6},{8,9},{9,8},{10,11... | collective-permute-start | bytes 1572872 | tf_op jit(solution)/shard_map/ppermute | solution.py:472
Sparse Core Ops, SparseCore 0:
  27.4 69.7 all-gather.3
